TPU v7x, 256 devices: a 2x2x32 block of a 4x8x32 slice. The times are simulated.
256 devices in a mesh: grp: 4 (over y, x), ep: 64 (over z, core).
Axes of the slice: x: 2, y: 2, z: 32, core: 2. Of those that a mesh axis runs over, the one named last changes fastest.
The devices are a block of a 4x8x32 slice.
Arguments:
- tokens: bfloat16 [1024, 2048], P(('grp', 'ep')), parts along dimension 0, may hold values from -6 to 6
- prior_state: float32 [1024, 32, 64, 64], P(('grp', 'ep')), parts along dimension 0, may hold values from -3 to 3
- receptance_matrix: bfloat16 [2048, 2048], P('ep'), may hold values from -0.125 to 0.125
- key_matrix: bfloat16 [2048, 2048], P('ep'), may hold values from -0.125 to 0.125
- value_matrix: bfloat16 [2048, 2048], P('ep'), may hold values from -0.125 to 0.125
- decay_lowrank_first: bfloat16 [2048, 64], replicated, may hold values from -0.125 to 0.125
- decay_lowrank_second: bfloat16 [64, 2048], replicated, may hold values from -1.5 to 1.5
- decay_channel_offset: float32 [2048], replicated, may hold values from -6 to 0
- correction_lowrank_first: bfloat16 [2048, 64], replicated, may hold values from -0.125 to 0.125
- correction_lowrank_second: bfloat16 [64, 2048], replicated, may hold values from -1.5 to 1.5
- correction_offset: float32 [2048], replicated, may hold values from -4 to 4
- gate_lowrank_first: bfloat16 [2048, 128], replicated, may hold values from -0.25 to 0.25
- gate_lowrank_second: bfloat16 [128, 2048], replicated, may hold values from -0.5 to 0.5
- key_rate_blend: float32 [2048], replicated, may hold values from 0.1 to 1.9
- self_token_scale: float32 [32, 64], replicated, may hold values from -1.2 to 1.2
- per_head_gain: float32 [2048], replicated, may hold values from 0.1 to 1.9
- per_head_bias: float32 [2048], replicated, may hold values from -1.8 to 1.8
- mixer_output_weight: bfloat16 [2048, 2048], P('ep'), may hold values from -0.125 to 0.125
- mixer_norm_gain: float32 [2048], replicated, may hold values from 0.1 to 1.9
- mixer_norm_bias: float32 [2048], replicated, may hold values from -1.8 to 1.8
- expert_norm_gain: float32 [2048], replicated, may hold values from 0.1 to 1.9
- expert_norm_bias: float32 [2048], replicated, may hold values from -1.8 to 1.8
- routes: int32 [1024, 4], P(('grp', 'ep')), parts along dimension 0, may hold values from 0 to 63, all different within a row; in each aligned block of 4 rows (0 to 3, 4 to 7, ...) at most 2 rows name the same one
- routing_weight: float32 [1024, 4], P(('grp', 'ep')), parts along dimension 0, may hold values from 0.1 to 1
- expert_gate_weight: bfloat16 [64, 2048, 512], P('ep'), may hold values from -0.125 to 0.125
- expert_up_weight: bfloat16 [64, 2048, 512], P('ep'), may hold values from -0.125 to 0.125
- expert_down_weight: bfloat16 [64, 512, 2048], P('ep'), may hold values from -0.25 to 0.25
Outputs:
- result: bfloat16 [1024, 2048], P(('grp', 'ep')), parts along dimension 0
- next_state: float32 [1024, 32, 64, 64], P(('grp', 'ep')), parts along dimension 0
There are 4 independent parts, one for each index of `grp`. A program takes and returns all parts, laid end to end along the dimension named above; an argument that names none is the same for every part. Nothing has to cross between parts.
Inputs may be any that keep to these rules, and one draw needn't show every extreme that they name: `routes`: A row names 4 different experts. Among the rows of one device no expert is named more than 2 times, and in some device one expert is named exactly 2 times; every expert is named somewhere.
All inputs are finite; a program needn't handle non-finite values.
Results may differ from a plain program's by a relative error of at most 0.0081.
Values may be sent and summed in bfloat16 or wider, within the bound.
A program may use at most 128 MiB of HBM per device.

v0:
```python
import jax
import jax.numpy as jnp
from jax import lax
from jax.sharding import PartitionSpec as P


def side_by_side(arrays, axis, dim, along):
    widths = [a.shape[along] for a in arrays]
    both = jnp.concatenate(arrays, axis=along)
    whole = lax.all_gather(both, axis, axis=dim, tiled=True)
    return tuple(jnp.split(whole, [sum(widths[:k]) for k in range(1, len(widths))], axis=along))


def cut_along(value, dim, devices):
    shape = value.shape
    parts = value.reshape(*shape[:dim], devices, shape[dim] // devices, *shape[dim + 1 :])
    return jnp.moveaxis(parts, dim, 0)


def summed_on_arrival(value, axis, dim):
    devices = lax.axis_size(axis)
    parts = lax.all_to_all(cut_along(value, dim, devices), axis, 0, 0, tiled=True)
    return jnp.sum(parts.astype(jnp.float32), axis=0)


def layer_norm(values_in, gain_vec, bias_vec):
    row_mean = jnp.mean(values_in, -1, keepdims=True)
    centered = values_in - row_mean
    row_var = jnp.mean(centered * centered, -1, keepdims=True)
    return centered * lax.rsqrt(row_var + 1e-05) * gain_vec + bias_vec


def recurrent_readout(
    tokens,
    prior_state,
    receptance_rows,
    key_rows,
    value_rows,
    decay_lowrank_first,
    decay_lowrank_second,
    decay_channel_offset,
    correction_lowrank_first,
    correction_lowrank_second,
    correction_offset,
    gate_lowrank_first,
    gate_lowrank_second,
    key_rate_blend,
    self_token_scale,
    per_head_gain,
    per_head_bias,
):
    row_count = tokens.shape[0]
    head_count = prior_state.shape[1]
    head_size = prior_state.shape[2]
    squash = jnp.tanh(
        jnp.dot(tokens, decay_lowrank_first, preferred_element_type=jnp.float32)
    ).astype(jnp.bfloat16)
    pre_decay = decay_channel_offset + jnp.dot(
        squash, decay_lowrank_second, preferred_element_type=jnp.float32
    )
    decay_rate = jnp.exp(-jnp.exp(-jax.nn.softplus(-pre_decay) - 0.5))
    low_learn = jnp.dot(
        tokens, correction_lowrank_first, preferred_element_type=jnp.float32
    ).astype(jnp.bfloat16)
    learn_rate = jax.nn.sigmoid(
        correction_offset
        + jnp.dot(low_learn, correction_lowrank_second, preferred_element_type=jnp.float32)
    )
    opened = jax.nn.sigmoid(
        jnp.dot(tokens, gate_lowrank_first, preferred_element_type=jnp.float32)
    ).astype(jnp.bfloat16)
    gating = jnp.dot(opened, gate_lowrank_second, preferred_element_type=jnp.float32)

    def by_head(flat_arr):
        return flat_arr.reshape(row_count, head_count, head_size)

    scaled = by_head(key_rows)
    unit_key = scaled * lax.rsqrt(jnp.sum(scaled * scaled, -1, keepdims=True) + 1e-06)
    written_key = by_head(key_rows * (1.0 + (learn_rate - 1.0) * key_rate_blend))
    receptance_by_head = by_head(receptance_rows)
    value_by_head = by_head(value_rows)
    removed = jnp.einsum("nhvk,nhk->nhv", prior_state, unit_key, precision=lax.Precision.HIGHEST)
    next_state = (
        prior_state * by_head(decay_rate)[:, :, None, :]
        - removed[..., None] * (unit_key * by_head(learn_rate))[:, :, None, :]
        + value_by_head[..., None] * written_key[:, :, None, :]
    )
    readout = jnp.einsum(
        "nhvk,nhk->nhv", next_state, receptance_by_head, precision=lax.Precision.HIGHEST
    )
    head_mean = jnp.mean(readout, -1, keepdims=True)
    head_dev = readout - head_mean
    head_var = jnp.mean(head_dev * head_dev, -1, keepdims=True)
    normed = (head_dev * lax.rsqrt(head_var + 0.00064)).reshape(
        row_count, -1
    ) * per_head_gain + per_head_bias
    self_token_term = (
        jnp.sum(receptance_by_head * written_key * self_token_scale, -1, keepdims=True)
        * value_by_head
    )
    mixer_result = ((normed + self_token_term.reshape(row_count, -1)) * gating).astype(jnp.bfloat16)
    return (mixer_result, next_state)


def body(
    tokens,
    prior_state,
    receptance_matrix,
    key_matrix,
    value_matrix,
    decay_lowrank_first,
    decay_lowrank_second,
    decay_channel_offset,
    correction_lowrank_first,
    correction_lowrank_second,
    correction_offset,
    gate_lowrank_first,
    gate_lowrank_second,
    key_rate_blend,
    self_token_scale,
    per_head_gain,
    per_head_bias,
    mixer_output_weight,
    mixer_norm_gain,
    mixer_norm_bias,
    expert_norm_gain,
    expert_norm_bias,
    routes,
    routing_weight,
    expert_gate_weight,
    expert_up_weight,
    expert_down_weight,
):
    own_rows = tokens.shape[0]
    shard_rows = side_by_side((receptance_matrix, key_matrix, value_matrix), "ep", 0, 1)
    segment = tokens
    receptance_rows, key_rows, value_rows = tuple(
        (
            jnp.dot(segment, weight_mat, preferred_element_type=jnp.float32)
            for weight_mat in shard_rows
        )
    )
    mixer_result, next_state = recurrent_readout(
        tokens,
        prior_state,
        receptance_rows,
        key_rows,
        value_rows,
        decay_lowrank_first,
        decay_lowrank_second,
        decay_channel_offset,
        correction_lowrank_first,
        correction_lowrank_second,
        correction_offset,
        gate_lowrank_first,
        gate_lowrank_second,
        key_rate_blend,
        self_token_scale,
        per_head_gain,
        per_head_bias,
    )
    mixer_cols = lax.all_to_all(mixer_result, "ep", split_axis=1, concat_axis=0, tiled=True)
    segment = mixer_cols
    mixed = summed_on_arrival(
        jnp.dot(segment, mixer_output_weight, preferred_element_type=jnp.float32).astype(
            jnp.bfloat16
        ),
        "ep",
        0,
    )
    hidden = layer_norm(
        tokens.astype(jnp.float32) + mixed, mixer_norm_gain, mixer_norm_bias
    ).astype(jnp.bfloat16)
    model_width = hidden.shape[1]
    top_count = routes.shape[1]
    expert_count = lax.axis_size("ep")
    capacity = max(2, 2 * own_rows * top_count // expert_count)
    flat_ids = routes.reshape(-1)
    onehot = (flat_ids[:, None] == jnp.arange(expert_count, dtype=jnp.int32)[None, :]).astype(
        jnp.int32
    )
    earlier = jnp.cumsum(onehot, 0) - onehot
    slot_rank = jnp.sum(earlier * onehot, 1)
    target = flat_ids * capacity + slot_rank
    dispatch = (
        target[:, None] == jnp.arange(expert_count * capacity, dtype=jnp.int32)[None, :]
    ).astype(jnp.bfloat16)
    repeated = jnp.repeat(hidden, top_count, axis=0)
    outgoing = lax.dot_general(
        dispatch, repeated, (((0,), (0,)), ((), ())), preferred_element_type=jnp.float32
    ).astype(jnp.bfloat16)
    outgoing = outgoing.reshape(expert_count, capacity, model_width)
    arrived = lax.all_to_all(outgoing, "ep", split_axis=0, concat_axis=0, tiled=True)
    sources, slot_count, width_in = arrived.shape
    flat_in = arrived.reshape(sources * slot_count, width_in)
    gate_val = jnp.dot(flat_in, expert_gate_weight[0], preferred_element_type=jnp.float32)
    up_val = jnp.dot(flat_in, expert_up_weight[0], preferred_element_type=jnp.float32)
    inner = (jax.nn.silu(gate_val) * up_val).astype(jnp.bfloat16)
    produced = jnp.dot(inner, expert_down_weight[0], preferred_element_type=jnp.float32).astype(
        jnp.bfloat16
    )
    returned = lax.all_to_all(
        produced.reshape(sources, slot_count, width_in),
        "ep",
        split_axis=0,
        concat_axis=0,
        tiled=True,
    )
    picked = jnp.dot(
        dispatch,
        returned.reshape(expert_count * capacity, model_width),
        preferred_element_type=jnp.float32,
    )
    share = routing_weight / jnp.sum(routing_weight, -1, keepdims=True)
    combined = jnp.sum(picked.reshape(own_rows, top_count, model_width) * share[..., None], 1)
    result = layer_norm(
        hidden.astype(jnp.float32) + combined, expert_norm_gain, expert_norm_bias
    ).astype(jnp.bfloat16)
    return (result, next_state)


def solution(mesh):
    in_specs = (
        P(("grp", "ep"), None),
        P(("grp", "ep"), None, None, None),
        P("ep", None),
        P("ep", None),
        P("ep", None),
        P(),
        P(),
        P(),
        P(),
        P(),
        P(),
        P(),
        P(),
        P(),
        P(),
        P(),
        P(),
        P("ep", None),
        P(),
        P(),
        P(),
        P(),
        P(("grp", "ep"), None),
        P(("grp", "ep"), None),
        P("ep", None, None),
        P("ep", None, None),
        P("ep", None, None),
    )
    out_specs = (P(("grp", "ep"), None), P(("grp", "ep"), None, None, None))
    return jax.shard_map(body, mesh=mesh, in_specs=in_specs, out_specs=out_specs, check_vma=False)
```

profile of v0, /device:TPU:46, one launch (start us, length us, event | category | flops | bytes accessed | tf_op | source)
XLA Modules:
  0.0 539.7 jit_solution(7225675819815774377)
XLA Ops:
  7.3 1.9 pad_maximum_fusion
  9.3 1.4 fusion.19
  10.8 1.5 fusion.52
  12.4 172.3 %all-gather.2.cloned.1.call-done = bf16[2048,6144]{1,0:T(8,128)(2,1)} async-done(((bf16[32,6144]{1,0:T(8,128)(2,1)}), bf16[2048,6144]{1,0:T(8,128)(2,1)}) %all-gather.2.cloned.1.call-update) | async-done | bytes 25165840 | tf_op jit(solution)/shard_map/all_gather | solution.py:10
  184.7 4.6 fusion.13
  189.5 4.6 add_multiply_fusion
  194.4 4.6 fusion.10
  199.4 8.7 %fusion.66 = f32[4,32,1,64]{3,2,1,0:T(1,128)S(1)} fusion(f32[4,32,64,1]{2,3,1,0:T(1,128)S(1)} %bitcast.62, f32[4,32,64,64]{3,2,1,0:T(8,128)} %param.28), kind=kOutput, calls=%fused_computation.93 | convolution fusion | flops 6291456 | bytes 2162688 | tf_op jit(solution)/shard_map/nhvk,nhk->nhv/dot_general | solution.py:82
  208.1 2.8 multiply_add_fusion
  210.9 2.0 copy-done.2
  212.9 6.6 %fusion.67 = f32[4,32,1,64]{3,2,1,0:T(1,128)S(1)} fusion(f32[4,32,64,64]{3,2,1,0:T(8,128)S(1)} %multiply_add_fusion, f32[4,32,64,1]{2,3,1,0:T(1,128)S(1)} %bitcast.61), kind=kOutput, calls=%fused_computation.94 | convolution fusion | flops 6291456 | bytes 2162688 | tf_op jit(solution)/shard_map/nhvk,nhk->nhv/dot_general | solution.py:88
  220.0 1.4 fusion.21
  221.6 42.3 %all_to_all.34 = bf16[4,64,32]{2,0,1:T(4,128)(2,1)S(1)} all-to-all(bf16[4,64,32]{2,0,1:T(4,128)(2,1)S(1)} %copy.30), channel_id=1, replica_groups=mesh['grp'=4,'ep'=64] {'ep'}, dimensions={1} | all-to-all | bytes 32768 | tf_op jit(solution)/shard_map/all_to_all | solution.py:162
  263.9 0.4 convolution_convert_fusion
  264.3 1.2 reshape.149
  265.5 6.7 %all-to-all-start.1 = ((bf16[64,4,2048]{2,1,0:T(4,128)(2,1)}), bf16[64,4,2048]{2,1,0:T(4,128)(2,1)S(1)}, u32[]{:S(2)}, u32[]{:S(2)}) async-start(bf16[64,4,2048]{2,1,0:T(4,128)(2,1)} %reshape.149), calls=%async_computation.1 | async-start | bytes 2097152 | tf_op jit(solution)/shard_map/all_to_all | solution.py:22
  272.7 108.6 %all-to-all-done.1 = bf16[64,4,2048]{2,1,0:T(4,128)(2,1)S(1)} async-done(((bf16[64,4,2048]{2,1,0:T(4,128)(2,1)}), bf16[64,4,2048]{2,1,0:T(4,128)(2,1)S(1)}, u32[]{:S(2)}, u32[]{:S(2)}) %all-to-all-start.1) | async-done | bytes 1048608 | tf_op jit(solution)/shard_map/all_to_all | solution.py:22
  381.3 0.4 convert_reduce_fusion
  381.9 0.2 multiply_reduce_fusion.4
  382.2 0.4 convolution_convert_fusion.2
  382.7 0.3 reshape.151
  383.0 70.6 %all_to_all.35 = bf16[64,2,2048]{2,1,0:T(2,128)(2,1)} all-to-all(bf16[64,2,2048]{2,1,0:T(2,128)(2,1)S(1)} %reshape.151), channel_id=1, replica_groups=mesh['grp'=4,'ep'=64] {'ep'}, dimensions={0} | all-to-all | bytes 1048576 | tf_op jit(solution)/shard_map/all_to_all | solution.py:193
  453.6 1.2 reshape.152
  454.8 2.0 fusion.25
  456.9 2.4 convolution_convert_fusion.1
  459.4 1.1 reshape.153
  460.5 6.5 %all-to-all-start.3 = ((bf16[64,2,2048]{2,1,0:T(2,128)(2,1)}), bf16[64,2,2048]{2,1,0:T(2,128)(2,1)S(1)}, u32[]{:S(2)}, u32[]{:S(2)}) async-start(bf16[64,2,2048]{2,1,0:T(2,128)(2,1)} %reshape.153), calls=%async_computation.3 | async-start | bytes 1048576 | tf_op jit(solution)/shard_map/all_to_all | solution.py:202
  467.3 64.0 %all-to-all-done.3 = bf16[64,2,2048]{2,1,0:T(2,128)(2,1)S(1)} async-done(((bf16[64,2,2048]{2,1,0:T(2,128)(2,1)}), bf16[64,2,2048]{2,1,0:T(2,128)(2,1)S(1)}, u32[]{:S(2)}, u32[]{:S(2)}) %all-to-all-start.3) | async-done | bytes 524320 | tf_op jit(solution)/shard_map/all_to_all | solution.py:202
  531.2 0.2 reshape.159
  531.4 0.3 fusion.35
  531.9 0.2 multiply_reduce_fusion.3
  532.1 0.7 add_convert_fusion
  (71 shorter events, 3.0 us)
Async XLA Ops:
  7.2 449.7 %copy-start = (bf16[1,512,2048]{2,1,0:T(8,128)(2,1)S(1)}, bf16[1,512,2048]{2,1,0:T(8,128)(2,1)}, u32[]{:S(2)}) copy-start(bf16[1,512,2048]{2,1,0:T(8,128)(2,1)} %param.53) | copy-start | bytes 6291460
  7.2 177.5 %all-gather.2.cloned.1.call-start = ((), (), s32[]{:S(2)}) async-start(), calls=%async_computation.4 | async-start | bytes 25559040 | tf_op jit(solution)/shard_map/all_gather | solution.py:10
  12.4 177.1 %copy-start.3 = (bf16[4,2048]{1,0:T(4,128)(2,1)S(1)}, bf16[4,2048]{1,0:T(4,128)(2,1)}, u32[]{:S(2)}) copy-start(bf16[4,2048]{1,0:T(4,128)(2,1)} %param.27) | copy-start | bytes 49156
  12.4 177.1 %copy-start.15 = (f32[2048]{0:T(1024)S(1)}, f32[2048]{0:T(1024)}, u32[]{:S(2)}) copy-start(f32[2048]{0:T(1024)} %param.40) | copy-start | bytes 24580
  189.5 4.7 copy-start.6
  199.2 8.9 %copy-start.1 = (f32[4,32,64,64]{3,2,1,0:T(8,128)S(1)}, f32[4,32,64,64]{3,2,1,0:T(8,128)}, u32[]{:S(2)}) copy-start(f32[4,32,64,64]{3,2,1,0:T(8,128)} %param.28) | copy-start | bytes 6291460
  210.8 2.0 copy-start.2
  210.9 9.1 %copy-start.4 = (bf16[128,2048]{1,0:T(8,128)(2,1)S(1)}, bf16[128,2048]{1,0:T(8,128)(2,1)}, u32[]{:S(2)}) copy-start(bf16[128,2048]{1,0:T(8,128)(2,1)} %param.39) | copy-start | bytes 1572868
  210.9 9.1 %copy-start.7 = (f32[2048]{0:T(1024)S(1)}, f32[2048]{0:T(1024)}, u32[]{:S(2)}) copy-start(f32[2048]{0:T(1024)} %param.43) | copy-start | bytes 24580
  210.9 9.1 %copy-start.8 = (f32[2048]{0:T(1024)S(1)}, f32[2048]{0:T(1024)}, u32[]{:S(2)}) copy-start(f32[2048]{0:T(1024)} %param.42) | copy-start | bytes 24580
  210.9 53.0 %copy-start.5 = (bf16[32,2048]{1,0:T(8,128)(2,1)S(1)}, bf16[32,2048]{1,0:T(8,128)(2,1)}, u32[]{:S(2)}) copy-start(bf16[32,2048]{1,0:T(8,128)(2,1)} %param.44) | copy-start | bytes 393220
  219.4 52.8 %copy-start.9 = (s32[4,4]{1,0:T(4,128)S(1)}, s32[4,4]{1,0:T(4,128)}, u32[]{:S(2)}) copy-start(s32[4,4]{1,0:T(4,128)} %param.49) | copy-start | bytes 196
  219.7 162.3 %copy-start.11 = (f32[2048]{0:T(1024)S(1)}, f32[2048]{0:T(1024)}, u32[]{:S(2)}) copy-start(f32[2048]{0:T(1024)} %param.46) | copy-start | bytes 24580
  219.8 162.3 %copy-start.12 = (f32[2048]{0:T(1024)S(1)}, f32[2048]{0:T(1024)}, u32[]{:S(2)}) copy-start(f32[2048]{0:T(1024)} %param.45) | copy-start | bytes 24580
  265.5 115.8 %all-to-all-start.1 = ((bf16[64,4,2048]{2,1,0:T(4,128)(2,1)}), bf16[64,4,2048]{2,1,0:T(4,128)(2,1)S(1)}, u32[]{:S(2)}, u32[]{:S(2)}) async-start(bf16[64,4,2048]{2,1,0:T(4,128)(2,1)} %reshape.149), calls=%async_computation.1 | async-start | bytes 2097152 | tf_op jit(solution)/shard_map/all_to_all | solution.py:22
  456.9 10.2 %copy-start.10 = (f32[4,4]{1,0:T(4,128)S(1)}, f32[4,4]{1,0:T(4,128)}, u32[]{:S(2)}) copy-start(f32[4,4]{1,0:T(4,128)} %param.50) | copy-start | bytes 196
  456.9 75.2 %copy-start.13 = (f32[2048]{0:T(1024)S(1)}, f32[2048]{0:T(1024)}, u32[]{:S(2)}) copy-start(f32[2048]{0:T(1024)} %param.48) | copy-start | bytes 24580
  456.9 75.2 %copy-start.14 = (f32[2048]{0:T(1024)S(1)}, f32[2048]{0:T(1024)}, u32[]{:S(2)}) copy-start(f32[2048]{0:T(1024)} %param.47) | copy-start | bytes 24580
  460.5 70.7 %all-to-all-start.3 = ((bf16[64,2,2048]{2,1,0:T(2,128)(2,1)}), bf16[64,2,2048]{2,1,0:T(2,128)(2,1)S(1)}, u32[]{:S(2)}, u32[]{:S(2)}) async-start(bf16[64,2,2048]{2,1,0:T(2,128)(2,1)} %reshape.153), calls=%async_computation.3 | async-start | bytes 1048576 | tf_op jit(solution)/shard_map/all_to_all | solution.py:202
Sparse Core Ops, SparseCore 0:
  10.5 174.2 all-gather.1
where the time goes:
time: 541 us; the launch traced here: 540 us
  waiting for transfers between devices  345 us (64%)
  blocking collectives  113 us (21%)
  matrix products  38.9 us (7%)
  between operations  14.4 us (3%)
  starting transfers between devices  13.3 us (2%)
  other arithmetic  7.77 us (1%)
  local copies, waits for them, and re-layouts  7.44 us (1%)
    all_gather x1, waiting for transfers between devices, side_by_side(): whole = lax.all_gather(both, axis, axis=dim, tiled=True)  172 us
    all_to_all x1, waiting for transfers between devices, summed_on_arrival(): lax.all_to_all(cut_along(value, dim, devices), axis, 0, 0, tiled=True)  109 us
    all_to_all x1, blocking collectives, body(): lax.all_to_all(outgoing, 'ep', split_axis=0, concat_axis=0, tiled=True)  70.6 us
    all_to_all x1, waiting for transfers between devices, body(): lax.all_to_all(produced.reshape(sources, slot_count, width_in), 'ep', spl...  64 us
    all_to_all x1, blocking collectives, body(): lax.all_to_all(mixer_result, 'ep', split_axis=1, concat_axis=0, tiled=True)  42.3 us
    dot_general x3, matrix products, body(): jnp.dot(segment, weight_mat, preferred_element_type=jnp.float32)  13.7 us
  transfers between devices with their start and end apart: 3, of which 3 were waited for; matrix products, arithmetic and copies ran while one was open for 1% of the time, Pallas kernels for 0%

commit v1 on v0

v1 whole, which is shorter than its diff:
```python
import functools

import jax
import jax.numpy as jnp
from jax import lax
from jax.experimental import pallas as pl
from jax.experimental.pallas import tpu as pltpu
from jax.sharding import PartitionSpec as P

MESH = pl.DeviceIdType.MESH
F32 = jnp.float32
BF16 = jnp.bfloat16
ROWS = 4
HEAD = 64
STRIDE = 4


def dot(a, b):
    return jnp.dot(a, b, preferred_element_type=F32)


def lane_ids(shape):
    return lax.broadcasted_iota(jnp.int32, shape, len(shape) - 1)


def row_ids(shape):
    return lax.broadcasted_iota(jnp.int32, shape, len(shape) - 2)


def kernel(
    nz,
    share,
    ff,
    tok_ref,
    state_hbm,
    wr_hbm,
    wk_hbm,
    wv_hbm,
    wo_hbm,
    dl1,
    dl2,
    doff,
    cl1,
    cl2,
    coff,
    gl1,
    gl2,
    blend,
    sscale,
    hgain,
    hbias,
    mgain,
    mbias,
    egain,
    ebias,
    routes,
    rweight,
    eg_hbm,
    eu_hbm,
    ed_hbm,
    out_ref,
    next_hbm,
    st,
    wstage,
    wsend,
    wb,
    em,
    xt,
    xm,
    xh,
    ysend,
    yrecv,
    msend,
    mrecv,
    cb,
    csend,
    tok8,
    tokp,
    hidp,
    dh,
    ah,
    gh,
    ro,
    sv,
    eg,
    eu,
    ed,
    zown,
    zoth,
    zsib,
    tsum,
    r1,
    u2,
    r2,
    ld_sem,
    w_send,
    w_recv,
    q_send,
    q_recv,
    s_send,
    s_recv,
    l1_send,
    l1_recv,
    l2_send,
    l2_recv,
    a_send,
    a_recv,
    x_send,
    x_recv,
    f1_send,
    f1_recv,
    f2_send,
    f2_recv,
    bar_wait_dummy,
):
    nk = nz // STRIDE
    dim = HEAD * nz
    half = dim // 2
    nm = 4 // share
    ep = lax.axis_index("ep")
    grp = lax.axis_index("grp")
    z = ep // 2
    c = ep % 2
    gq = grp % share
    gbase = grp - gq
    res = z % STRIDE
    own_k = z // STRIDE
    sib = {"ep": z * 2 + 1 - c}

    def chip(zt):
        return {"ep": (zt % nz) * 2 + c}

    def slot_of(zt):
        return (zt % STRIDE) * nk + zt // STRIDE

    def far_first(j):
        d = nz // 2 - (j + 1) // 2
        return (z + nz + d * (1 - 2 * (j % 2))) % nz

    bar = pltpu.get_barrier_semaphore()

    @pl.loop(1, nz)
    def _(j):
        pl.semaphore_signal(bar, inc=1, device_id=chip(z + j), device_id_type=MESH)

    pl.semaphore_signal(bar, inc=1, device_id=sib, device_id_type=MESH)
    for i in range(1, share):
        pl.semaphore_signal(
            bar, inc=1, device_id={"grp": gbase + (gq + i) % share}, device_id_type=MESH
        )

    w_hbm = (wr_hbm, wk_hbm, wv_hbm, wo_hbm)
    for i in range(nm):
        for m in range(4):
            if m % nm == i:

                @pl.when(gq == m // nm)
                def _(i=i, m=m):
                    pltpu.make_async_copy(w_hbm[m], wstage.at[i], ld_sem.at[i]).start()

    st_load = pltpu.make_async_copy(state_hbm, st, ld_sem.at[4])
    eg_load = pltpu.make_async_copy(eg_hbm.at[0], eg, ld_sem.at[5])
    eu_load = pltpu.make_async_copy(eu_hbm.at[0], eu, ld_sem.at[6])
    ed_load = pltpu.make_async_copy(ed_hbm.at[0], ed, ld_sem.at[7])
    st_load.start()
    eg_load.start()
    eu_load.start()
    ed_load.start()

    lane128 = lane_ids((8, 128))
    left = lane128 < HEAD
    top = row_ids((8, 128)) < ROWS
    lane16 = lane_ids((16, 128))
    left16 = lane16 < HEAD

    tok = tok_ref[...].astype(F32)
    tok8[0:ROWS, :] = tok
    tok8[ROWS : 2 * ROWS, :] = tok
    tokp[0:ROWS, :] = tok[:, :half]
    tokp[ROWS : 2 * ROWS, :] = tok[:, half:]
    xt[res, own_k] = tokp[...].astype(BF16)

    for i in range(nm):
        pltpu.make_async_copy(w_hbm[0], wstage.at[i], ld_sem.at[i]).wait()

        @pl.loop(0, nz // 2)
        def _(t, i=i):
            at = pl.multiple_of(t * 128, 128)
            a = wstage[i, 0:16, pl.ds(at, 128)].astype(F32)
            b = wstage[i, 16:32, pl.ds(at, 128)].astype(F32)
            wsend[i, 2 * t] = jnp.where(left16, a, pltpu.roll(b, HEAD, 1)).astype(BF16)
            wsend[i, 2 * t + 1] = jnp.where(left16, pltpu.roll(a, HEAD, 1), b).astype(BF16)

        wb[gq * nm + i, c, z] = wsend[i, z]

    weight = rweight[...]
    part = weight / jnp.sum(weight, -1, keepdims=True)
    ids = routes[...]
    lanes4 = lane_ids((ROWS, 128))
    by_expert = jnp.zeros((ROWS, 128), F32)
    for k in range(ids.shape[1]):
        by_expert += jnp.where(ids[:, k : k + 1] == lanes4, part[:, k : k + 1], 0.0)
    high = by_expert.astype(BF16).astype(F32)
    low = by_expert - high
    both = jnp.where(lanes4 < HEAD, high, pltpu.roll(low, HEAD, 1))
    sv[0, 0:ROWS, :] = both
    sv[0, ROWS : 2 * ROWS, :] = both
    csend[...] = sv[0].astype(BF16)
    my_slot = slot_of(z)
    cb[c, my_slot] = csend[...]

    def gather_start(buf, n):
        for d in [nk // 2] + [x for y in range(nk // 2 - 1, 0, -1) for x in (y, nk - y)]:
            kt = (own_k + d) % nk
            pltpu.make_async_remote_copy(
                src_ref=buf.at[res, own_k],
                dst_ref=buf.at[res, own_k],
                send_sem=l1_send.at[n, d],
                recv_sem=l1_recv.at[n, nk - d],
                device_id=chip(kt * STRIDE + res),
                device_id_type=MESH,
            ).start()

    def level_two(buf, n):
        hk = nk // 2
        up, down, far = (res + 1) % STRIDE, (res + STRIDE - 1) % STRIDE, (res + 2) % STRIDE
        steps = (
            (1, buf.at[res], buf.at[down]),
            (nz - 1, buf.at[res], buf.at[up]),
            (2, buf.at[res, pl.ds(0, hk)], buf.at[far, pl.ds(0, hk)]),
            (nz - 2, buf.at[res, pl.ds(hk, hk)], buf.at[far, pl.ds(hk, hk)]),
        )
        sends, recvs = [], []
        for i, (d, src, arrives) in enumerate(steps):
            sends.append(
                pltpu.make_async_remote_copy(
                    src_ref=src,
                    dst_ref=src,
                    send_sem=l2_send.at[n, i],
                    recv_sem=l2_recv.at[n, i],
                    device_id=chip(z + d),
                    device_id_type=MESH,
                )
            )
            recvs.append(
                pltpu.make_async_remote_copy(
                    src_ref=arrives,
                    dst_ref=arrives,
                    send_sem=l2_send.at[n, i],
                    recv_sem=l2_recv.at[n, i],
                    device_id=chip(z + d),
                    device_id_type=MESH,
                )
            )
        return sends, recvs

    def gather_relay(buf, n):
        for d in range(1, nk):
            at = buf.at[res, (own_k + d) % nk]
            pltpu.make_async_remote_copy(
                src_ref=at,
                dst_ref=at,
                send_sem=l1_send.at[n, d],
                recv_sem=l1_recv.at[n, d],
                device_id=chip(z),
                device_id_type=MESH,
            ).wait_recv()
        sends, _ = level_two(buf, n)
        for s in sends:
            s.start()

    def gather_wait(buf, n):
        _, recvs = level_two(buf, n)
        for r in recvs:
            r.wait_recv()

    def gather_drain(buf, n):
        for d in range(1, nk):
            at = buf.at[res, own_k]
            pltpu.make_async_remote_copy(
                src_ref=at,
                dst_ref=at,
                send_sem=l1_send.at[n, d],
                recv_sem=l1_recv.at[n, d],
                device_id=chip(z),
                device_id_type=MESH,
            ).wait_send()
        sends, _ = level_two(buf, n)
        for s in sends:
            s.wait_send()

    def scatter(src_of, dst, send_sem, recv_sem):
        @pl.loop(0, nz - 1)
        def _(j):
            zt = far_first(j)
            pltpu.make_async_remote_copy(
                src_ref=src_of(zt),
                dst_ref=dst,
                send_sem=send_sem,
                recv_sem=recv_sem,
                device_id=chip(zt),
                device_id_type=MESH,
            ).start()

    def scatter_all(block, send_sem, recv_sem):
        return pltpu.make_async_remote_copy(
            src_ref=block.at[pl.ds(0, nz - 1)],
            dst_ref=block.at[pl.ds(0, nz - 1)],
            send_sem=send_sem,
            recv_sem=recv_sem,
            device_id=chip(z),
            device_id_type=MESH,
        )

    pl.semaphore_wait(bar, nz - 1 + 1 + share - 1)

    gather_start(xt, 0)
    for i in range(nm):
        m = gq * nm + i
        scatter(lambda zt, i=i: wsend.at[i, zt], wb.at[m, c, z], w_send.at[i], w_recv.at[i])

    tokb = tok8[...].astype(BF16)
    squash = jnp.tanh(dot(tokb, dl1[...])).astype(BF16)
    lowl = dot(tokb, cl1[...]).astype(BF16)
    opened = jax.nn.sigmoid(dot(tokb, gl1[...])).astype(BF16)

    for j in range(nz // 2):
        cols = slice(128 * j, 128 * j + 128)

        def two_heads(ref, tile, j=j):
            ref[2 * j] = tile
            ref[2 * j + 1] = pltpu.roll(tile, HEAD, 1)

        pre = doff[:, cols] + dot(squash, dl2[:, cols])
        two_heads(dh, jnp.exp(-(jnp.exp(jnp.full((8, 128), -0.5, F32)) * jax.nn.sigmoid(pre))))
        two_heads(ah, jax.nn.sigmoid(coff[:, cols] + dot(lowl, cl2[:, cols])))
        two_heads(gh, dot(opened, gl2[:, cols]))

    gather_relay(xt, 0)

    def slab(m, core, to, send_sem, recv_sem):
        return pltpu.make_async_remote_copy(
            src_ref=wb.at[m, core],
            dst_ref=wb.at[m, core],
            send_sem=send_sem,
            recv_sem=recv_sem,
            device_id=to,
            device_id_type=MESH,
        )

    for i in range(nm):
        m = gq * nm + i
        scatter_all(wb.at[m, c], w_send.at[i], w_recv.at[i]).wait_recv()
        for g in range(1, share):
            slab(
                m,
                c,
                {"grp": gbase + (gq + g) % share},
                q_send.at[g, i],
                q_recv.at[share - g, i],
            ).start()
        slab(m, c, sib, s_send.at[0, i], s_recv.at[0, i]).start()
    for g in range(1, share):
        for i in range(nm):
            m = ((gq + g) % share) * nm + i
            slab(m, c, sib, q_send.at[g, i], q_recv.at[g, i]).wait_recv()
            slab(m, c, sib, s_send.at[g, i], s_recv.at[g, i]).start()

    def widen(m, at):
        keep = left16.astype(F32).astype(BF16)
        drop = (1.0 - left16.astype(F32)).astype(BF16)
        for hk in range(2):

            @pl.loop(0, nz // 2)
            def _(zz, hk=hk):
                for core in range(2):
                    tile = wb[m, core, hk * (nz // 2) + zz]
                    base = pl.multiple_of(zz * 64 + core * 32, 32)
                    cols = slice(at + hk * 128, at + hk * 128 + 128)
                    em[pl.ds(base, 16), cols] = tile * keep
                    em[pl.ds(pl.multiple_of(base + 16, 16), 16), cols] = tile * drop

    def rows_of(value):
        return value.astype(F32).reshape(8 * nz, half).astype(BF16)

    top3 = row_ids((nz, 8, 128)) < ROWS
    left3 = lane_ids((nz, 8, 128)) < HEAD
    topw = (row_ids((8 * nz, 128)) % 8) < ROWS

    def fold(r):
        a = jnp.where(topw, r[:, 0:128], r[:, 128:256])
        a = (a + pltpu.roll(a, HEAD, 1)).reshape(nz, 8, 128)
        return a + pltpu.roll(a, ROWS, 1)

    for g in range(share):
        for i in range(nm):
            m = ((gq + g) % share) * nm + i
            slab(m, 1 - c, sib, s_send.at[g, i], s_recv.at[g, i]).wait_recv()

    for m in range(4):
        widen(m, m * 256)

    gather_wait(xt, 0)
    xv = rows_of(xt[...])
    cr = fold(dot(xv, em[:, 0:256]))
    ck = fold(dot(xv, em[:, 256:512]))
    cv = fold(dot(xv, em[:, 512:768]))
    ysend[...] = jnp.where(top3, jnp.where(left3, cr, ck), cv).astype(BF16)
    scatter(lambda zt: ysend.at[slot_of(zt)], yrecv.at[z], a_send.at[0], a_recv.at[0])
    yrecv[z] = ysend[my_slot]
    scatter(lambda zt: csend, cb.at[c, my_slot], a_send.at[2], a_recv.at[2])
    st_load.wait()
    scatter_all(yrecv, a_send.at[0], a_recv.at[0]).wait_recv()

    eye = (
        lax.broadcasted_iota(jnp.int32, (HEAD, HEAD), 0)
        == lax.broadcasted_iota(jnp.int32, (HEAD, HEAD), 1)
    ).astype(F32)

    def pick(ref, j):
        tile = jnp.broadcast_to(ref[:, 128 * j : 128 * j + 128], (8, 128))
        return tile, pltpu.roll(tile, HEAD, 1)

    blends, scales = [], []
    for j in range(nz // 2):
        blends += pick(blend, j)
        scales += pick(sscale, j)
    for h in range(nz):
        ro[h] = blends[h]
        sv[h] = scales[h]

    @pl.loop(0, nz)
    def _(h):
        y = yrecv[h].astype(F32)
        turned = pltpu.roll(y, ROWS, 0)
        rk = jnp.where(top, y, turned)
        v = jnp.where(top, turned, y)
        r = jnp.where(left, rk, 0.0)
        k = jnp.where(left, pltpu.roll(rk, HEAD, 1), 0.0)
        a = ah[h]
        unit = k * lax.rsqrt(jnp.sum(k * k, -1, keepdims=True) + 1e-06)
        written = k * (1.0 + (a - 1.0) * ro[h])
        ua = unit * a
        own = jnp.sum(r * written * sv[h], -1, keepdims=True)
        d = dh[h]
        sv[h] = own * v
        for t in range(ROWS):
            one = slice(t, t + 1)
            s = st[t, h]
            removed = jnp.sum(s * unit[one, 0:HEAD], -1, keepdims=True)
            vcol = jnp.sum(eye * v[one, 0:HEAD], -1, keepdims=True)
            n = s * d[one, 0:HEAD] - removed * ua[one, 0:HEAD] + vcol * written[one, 0:HEAD]
            st[t, h] = n
            rcol = jnp.sum(n * r[one, 0:HEAD], -1, keepdims=True)
            row = jnp.sum(eye * rcol, 0, keepdims=True)
            ro[h, t : t + 1, 0:HEAD] = row
            ro[h, ROWS + t : ROWS + t + 1, 0:HEAD] = row

    st_store = pltpu.make_async_copy(st, next_hbm, ld_sem.at[4])
    st_store.start()

    def mixer_head(h, gain, bias):
        x = jnp.where(left, ro[h], 0.0)
        mean = jnp.sum(x, -1, keepdims=True) * (1.0 / HEAD)
        dev = jnp.where(left, x - mean, 0.0)
        var = jnp.sum(dev * dev, -1, keepdims=True) * (1.0 / HEAD)
        normed = dev * lax.rsqrt(var + 0.00064) * gain + bias
        return (normed + sv[h]) * gh[h]

    def mixer_pair(j):
        g0, g1 = pick(hgain, j)
        b0, b1 = pick(hbias, j)
        one, two = mixer_head(2 * j, g0, b0), mixer_head(2 * j + 1, g1, b1)
        return jnp.where(left, one, pltpu.roll(two, HEAD, 1))

    for j in range(nz // 4):
        tile = jnp.where(top, mixer_pair(j), mixer_pair(nz // 4 + j))
        xm[res, own_k, :, 128 * j : 128 * j + 128] = tile.astype(BF16)

    gather_start(xm, 1)
    gather_relay(xm, 1)
    gather_wait(xm, 1)
    co = fold(dot(rows_of(xm[...]), em[:, 768:1024]))
    co_high = co.astype(BF16).astype(F32)
    msend[...] = jnp.where(top3, co_high, co - co_high).astype(BF16)
    scatter(lambda zt: msend.at[slot_of(zt)], mrecv.at[z], a_send.at[1], a_recv.at[1])
    mrecv[z] = msend[my_slot]

    scatter_all(cb.at[c], a_send.at[2], a_recv.at[2]).wait_recv()

    def to_sib(src, dst, n):
        return pltpu.make_async_remote_copy(
            src_ref=src,
            dst_ref=dst,
            send_sem=x_send.at[n],
            recv_sem=x_recv.at[n],
            device_id=sib,
            device_id_type=MESH,
        )

    to_sib(cb.at[c], cb.at[c], 0).start()

    scatter_all(mrecv, a_send.at[1], a_recv.at[1]).wait_recv()
    for j in range(nz // 4):

        def mixed_pair(p):
            one, two = mrecv[2 * p].astype(F32), mrecv[2 * p + 1].astype(F32)
            tile = jnp.where(left, one, two)
            return tile + pltpu.roll(tile, ROWS, 0)

        cols = slice(128 * j, 128 * j + 128)
        tokp[:, cols] += jnp.where(top, mixed_pair(j), mixed_pair(nz // 4 + j))

    topp = row_ids((8, half)) < ROWS

    def packed(ref):
        return jnp.where(topp, ref[:, 0:half], ref[:, half:dim])

    def row_total(x):
        s = jnp.broadcast_to(jnp.sum(x, -1, keepdims=True), (8, 128))
        s = s + pltpu.roll(s, ROWS, 0)
        return s[:, 0:1] * (1.0 / dim)

    def layer_norm(x, gain, bias):
        dev = x - row_total(x)
        var = row_total(dev * dev)
        return dev * lax.rsqrt(var + 1e-05) * packed(gain) + packed(bias)

    hidden = layer_norm(tokp[...], mgain, mbias).astype(BF16)
    hidp[...] = hidden.astype(F32)
    xh[c, res, own_k] = hidden
    mine = xh.at[c]
    gather_start(mine, 2)
    gather_relay(mine, 2)
    gather_wait(mine, 2)
    to_sib(xh.at[c], xh.at[c], 1).start()

    eg_load.wait()
    eu_load.wait()
    ed_load.wait()
    to_sib(cb.at[1 - c], cb.at[1 - c], 0).wait_recv()

    def wide_fold(a, b):
        width = a.shape[1]
        keep = (row_ids((8 * nz, width)) % 8) < ROWS
        x = jnp.where(keep, a, b).reshape(nz, 8, width)
        return (x + pltpu.roll(x, ROWS, 1)).reshape(8 * nz, width)

    def expert(core):
        xv = rows_of(xh[core])
        lane3 = lane_ids((nz, 8, 128))
        hit = (lane3 == ep) | (lane3 == ep + HEAD)
        coef = jnp.sum(jnp.where(hit, cb[core].astype(F32), 0.0), -1, keepdims=True)
        coef = coef.reshape(8 * nz, 1)
        gate = wide_fold(dot(xv, eg[0:half, :]), dot(xv, eg[half:dim, :]))
        up = wide_fold(dot(xv, eu[0:half, :]), dot(xv, eu[half:dim, :]))
        inner = (gate * jax.nn.sigmoid(gate) * up).astype(BF16)
        return inner, coef

    def down(inner, coef, j, width):
        a = dot(inner, ed[:, j * width : (j + 1) * width])
        b = dot(inner, ed[:, half + j * width : half + (j + 1) * width])
        keep = (row_ids((8 * nz, width)) % 8) < ROWS
        return (jnp.where(keep, a, b) * coef).reshape(STRIDE, nk, 8, width)

    width = min(256, half)
    inner, coef = expert(c)
    for j in range(half // width):
        zown[:, :, :, j * width : (j + 1) * width] = down(inner, coef, j, width).astype(BF16)
    to_sib(xh.at[1 - c], xh.at[1 - c], 1).wait_recv()
    inner, coef = expert(1 - c)
    for j in range(half // width):
        zoth[:, :, :, j * width : (j + 1) * width] = down(inner, coef, j, width).astype(BF16)
    to_sib(zoth, zsib, 2).start()
    to_sib(zoth, zsib, 2).wait_recv()
    tsum[...] = (zown[...].astype(F32) + zsib[...].astype(F32)).astype(BF16)

    hk = nk // 2
    up, down_, far = (res + 1) % STRIDE, (res + STRIDE - 1) % STRIDE, (res + 2) % STRIDE
    first = (
        (1, tsum.at[up], r1.at[0]),
        (nz - 1, tsum.at[down_], r1.at[1]),
        (2, tsum.at[far, pl.ds(0, hk)], r1.at[2, pl.ds(0, hk)]),
        (nz - 2, tsum.at[far, pl.ds(hk, hk)], r1.at[2, pl.ds(hk, hk)]),
    )
    copies = [
        pltpu.make_async_remote_copy(
            src_ref=src,
            dst_ref=dst,
            send_sem=f1_send.at[i],
            recv_sem=f1_recv.at[i],
            device_id=chip(z + d),
            device_id_type=MESH,
        )
        for i, (d, src, dst) in enumerate(first)
    ]
    for cp in copies:
        cp.start()
    for cp in copies:
        cp.wait_recv()
    u2[...] = (
        tsum[res].astype(F32)
        + r1[0].astype(F32)
        + r1[1].astype(F32)
        + r1[2].astype(F32)
    ).astype(BF16)

    def last(d):
        kt = (own_k + d) % nk
        return pltpu.make_async_remote_copy(
            src_ref=u2.at[kt],
            dst_ref=r2.at[nk - d],
            send_sem=f2_send.at[d],
            recv_sem=f2_recv.at[nk - d],
            device_id=chip(kt * STRIDE + res),
            device_id_type=MESH,
        )

    for d in [nk // 2] + [x for y in range(nk // 2 - 1, 0, -1) for x in (y, nk - y)]:
        last(d).start()
    total = hidp[...] + u2[own_k].astype(F32)
    for d in range(1, nk):
        pltpu.make_async_remote_copy(
            src_ref=r2.at[d],
            dst_ref=r2.at[d],
            send_sem=f2_send.at[d],
            recv_sem=f2_recv.at[d],
            device_id=chip(z),
            device_id_type=MESH,
        ).wait_recv()
    for d in range(1, nk):
        total = total + r2[d].astype(F32)
    y = layer_norm(total, egain, ebias)
    out_ref[:, 0:half] = y[0:ROWS, :].astype(BF16)
    out_ref[:, half:dim] = y[ROWS : 2 * ROWS, :].astype(BF16)

    gather_drain(xt, 0)
    gather_drain(xm, 1)
    gather_drain(mine, 2)
    for i in range(nm):
        scatter_all(wb.at[gq * nm + i, c], w_send.at[i], w_recv.at[i]).wait_send()
        slab(gq * nm + i, c, sib, s_send.at[0, i], s_recv.at[0, i]).wait_send()
        for g in range(1, share):
            slab(gq * nm + i, c, sib, q_send.at[g, i], q_recv.at[g, i]).wait_send()
            m = ((gq + g) % share) * nm + i
            slab(m, c, sib, s_send.at[g, i], s_recv.at[g, i]).wait_send()
    scatter_all(yrecv, a_send.at[0], a_recv.at[0]).wait_send()
    scatter_all(mrecv, a_send.at[1], a_recv.at[1]).wait_send()
    scatter_all(cb.at[c], a_send.at[2], a_recv.at[2]).wait_send()
    to_sib(cb.at[c], cb.at[c], 0).wait_send()
    to_sib(xh.at[c], xh.at[c], 1).wait_send()
    to_sib(zoth, zsib, 2).wait_send()
    for cp in copies:
        cp.wait_send()
    for d in range(1, nk):
        last(d).wait_send()
    st_store.wait()


def step(nz, share, *args):
    tokens, state = args[0], args[1]
    dim = tokens.shape[1]
    half = dim // 2
    nk = nz // STRIDE
    nm = 4 // share
    ff = args[24].shape[2]
    args = list(args)
    for i in (7, 10, 13, 14, 15, 16, 18, 19, 20, 21):
        args[i] = args[i].reshape(1, dim)
    order = [0, 1, 2, 3, 4, 17, 5, 6, 7, 8, 9, 10, 11, 12, 13, 14, 15, 16, 18, 19, 20, 21]
    order += [22, 23, 24, 25, 26]
    operands = [args[i] for i in order]
    in_hbm = {1, 2, 3, 4, 5, 24, 25, 26}
    vmem = pl.BlockSpec(memory_space=pltpu.VMEM)
    hbm = pl.BlockSpec(memory_space=pl.ANY)
    dma = pltpu.SemaphoreType.DMA
    heads = (nz, 8, 128)
    rows = (STRIDE, nk, 8, half)
    scratch = [
        pltpu.VMEM(state.shape, F32),
        pltpu.VMEM((nm, 32, dim), BF16),
        pltpu.VMEM((nm, nz, 16, 128), BF16),
        pltpu.VMEM((4, 2, nz, 16, 128), BF16),
        pltpu.VMEM((half, 1024), BF16),
        pltpu.VMEM(rows, BF16),
        pltpu.VMEM(rows, BF16),
        pltpu.VMEM((2,) + rows, BF16),
        pltpu.VMEM(heads, BF16),
        pltpu.VMEM(heads, BF16),
        pltpu.VMEM(heads, BF16),
        pltpu.VMEM(heads, BF16),
        pltpu.VMEM((2,) + heads, BF16),
        pltpu.VMEM((8, 128), BF16),
        pltpu.VMEM((8, dim), F32),
        pltpu.VMEM((8, half), F32),
        pltpu.VMEM((8, half), F32),
        pltpu.VMEM(heads, F32),
        pltpu.VMEM(heads, F32),
        pltpu.VMEM(heads, F32),
        pltpu.VMEM(heads, F32),
        pltpu.VMEM(heads, F32),
        pltpu.VMEM((dim, ff), BF16),
        pltpu.VMEM((dim, ff), BF16),
        pltpu.VMEM((ff, dim), BF16),
        pltpu.VMEM(rows, BF16),
        pltpu.VMEM(rows, BF16),
        pltpu.VMEM(rows, BF16),
        pltpu.VMEM(rows, BF16),
        pltpu.VMEM((3, nk, 8, half), BF16),
        pltpu.VMEM((nk, 8, half), BF16),
        pltpu.VMEM((nk, 8, half), BF16),
        dma((8,)),
        dma((nm,)),
        dma((nm,)),
        dma((share, nm)),
        dma((share, nm)),
        dma((share, nm)),
        dma((share, nm)),
        dma((3, nk)),
        dma((3, nk)),
        dma((3, 4)),
        dma((3, 4)),
        dma((3,)),
        dma((3,)),
        dma((3,)),
        dma((3,)),
        dma((4,)),
        dma((4,)),
        dma((nk,)),
        dma((nk,)),
        dma((1,)),
    ]
    return pl.pallas_call(
        functools.partial(kernel, nz, share, ff),
        out_shape=(
            jax.ShapeDtypeStruct(tokens.shape, BF16),
            jax.ShapeDtypeStruct(state.shape, F32),
        ),
        in_specs=[hbm if i in in_hbm else vmem for i in range(len(operands))],
        out_specs=(vmem, hbm),
        scratch_shapes=scratch,
        compiler_params=pltpu.CompilerParams(
            collective_id=0, has_side_effects=True, vmem_limit_bytes=56 * 1024 * 1024
        ),
    )(*operands)


def solution(mesh):
    nz = mesh.shape["ep"] // 2
    groups = mesh.shape["grp"]
    share = 4 if groups % 4 == 0 else 2 if groups % 2 == 0 else 1
    owned, split, copied = P(("grp", "ep"), None), P("ep", None), P()
    in_specs = (
        owned,
        P(("grp", "ep"), None, None, None),
        split,
        split,
        split,
        *([copied] * 12),
        split,
        *([copied] * 4),
        owned,
        owned,
        P("ep", None, None),
        P("ep", None, None),
        P("ep", None, None),
    )
    out_specs = (owned, P(("grp", "ep"), None, None, None))
    return jax.shard_map(
        functools.partial(step, nz, share),
        mesh=mesh,
        in_specs=in_specs,
        out_specs=out_specs,
        check_vma=False,
    )
```

time: 541 us -> 204 us (0.38)
  waiting for transfers between devices: 345 us -> 0 us
  Pallas kernels: 0 us -> 189 us
  blocking collectives: 113 us -> 0 us
  matrix products: 38.9 us -> 0 us
  between operations: 14.4 us -> 0.64 us
  starting transfers between devices: 13.3 us -> 0 us
  other arithmetic: 7.77 us -> 0 us
    pallas_call x0 -> x1, Pallas kernels: none -> 189 us  [step(): pl.pallas_call(functools.partial(kernel, nz, share, ff), out_shape=(jax.S...]
    all_to_all x2 -> x0, waiting for transfers between devices: 173 us -> none  [the longest x1 109 us: summed_on_arrival(): lax.all_to_all(cut_along(value, dim, devices), axis, 0, 0, tiled=True)]
    all_gather x1 -> x0, waiting for transfers between devices: 172 us -> none  [side_by_side(): whole = lax.all_gather(both, axis, axis=dim, tiled=True)]
    all_to_all x2 -> x0, blocking collectives: 113 us -> none  [the longest x1 70.6 us: body(): lax.all_to_all(outgoing, 'ep', split_axis=0, concat_axis=0, tiled=True)]
    dot_general x13 -> x0, matrix products: 38.9 us -> none  [the longest x3 13.7 us: body(): jnp.dot(segment, weight_mat, preferred_element_type=jnp.float32)]
    all_to_all x2 -> x0, starting transfers between devices: 13.2 us -> none  [the longest x1 6.73 us: summed_on_arrival(): lax.all_to_all(cut_along(value, dim, devices), axis, 0, 0, tiled=True)]
    unnamed x32 -> x4, local copies, waits for them, and re-layouts: 2.05 us -> 10 us
  transfers between devices with their start and end apart: 3 -> 0, of which waited for: 3 -> 0; matrix products, arithmetic and copies ran while one was open for 1% -> 0% of each run, Pallas kernels for 0% -> 0%
where the time goes in v1:
time: 204 us; the launch traced here: 201 us
  Pallas kernels  189 us (93%)
  local copies, waits for them, and re-layouts  11.4 us (6%)
    pallas_call x1, Pallas kernels, step(): pl.pallas_call(functools.partial(kernel, nz, share, ff), out_shape=(jax.S...  189 us
    unnamed x4, local copies, waits for them, and re-layouts  10 us

profile of v1, /device:TPU:46, one launch (start us, length us, event | category | flops | bytes accessed | tf_op | source)
XLA Modules:
  0.0 201.4 jit_solution(5492297932905928547)
XLA Ops:
  0.6 1.4 reshape.37.sscale
  2.0 2.0 copy.29.dl1
  4.0 1.9 copy.30.cl1
  5.9 189.4 %shard_map.266 = (bf16[4,2048]{1,0:T(4,128)(2,1)}, f32[4,32,64,64]{3,2,1,0:T(8,128)}) custom-call(bf16[4,2048]{1,0:T(4,128)(2,1)} %tok_ref.1, f32[4,32,64,64]{3,2,1,0:T(8,128)} %state_hbm.1, bf16[32,2048]{1,0:T(8,128)(2,1)} %wr_hbm.1, bf16[32,2048]{1,0:T(8,128)(2,1)} %wk_hbm.1, bf16[32,2048]{1,0:T(8,128)(2,1)} %wv_hbm.1, bf16[32,2048]{1,0:T(8,128)(2,1)} %wo_hbm.1, ...), custom_call_target="tpu_custom_call" | custom-call | tf_op jit(solution)/shard_map/pallas_call | solution.py:733
  195.3 1.3 copy.33
  196.6 4.8 %copy.34 = f32[4,32,64,64]{3,2,1,0:T(8,128)} copy(f32[4,32,64,64]{3,2,1,0:T(8,128)} %get-tuple-element.5) | data formatting | bytes 4194304

commit v2 on v1

--- a/solution.py
+++ b/solution.py
@@ -10,6 +10,7 @@
 MESH = pl.DeviceIdType.MESH
 F32 = jnp.float32
 BF16 = jnp.bfloat16
+SMALL = 18
 ROWS = 4
 HEAD = 64
 STRIDE = 4
@@ -30,37 +31,54 @@
 def kernel(
     nz,
     share,
-    ff,
-    tok_ref,
+    tok_hbm,
     state_hbm,
     wr_hbm,
     wk_hbm,
     wv_hbm,
     wo_hbm,
-    dl1,
-    dl2,
-    doff,
-    cl1,
-    cl2,
-    coff,
-    gl1,
-    gl2,
-    blend,
-    sscale,
-    hgain,
-    hbias,
-    mgain,
-    mbias,
-    egain,
-    ebias,
-    routes,
-    rweight,
+    *rest,
+):
+    small_hbm, rest = rest[:SMALL], rest[SMALL:]
+    run(nz, share, tok_hbm, state_hbm, (wr_hbm, wk_hbm, wv_hbm, wo_hbm), small_hbm, *rest)
+
+
+def run(
+    nz,
+    share,
+    tok_hbm,
+    state_hbm,
+    w_hbm,
+    small_hbm,
     eg_hbm,
     eu_hbm,
     ed_hbm,
     out_ref,
     next_hbm,
+    tok_ref,
+    *rest,
+):
+    small, rest = rest[:SMALL], rest[SMALL:]
+    work(nz, share, tok_hbm, state_hbm, w_hbm, small_hbm, eg_hbm, eu_hbm, ed_hbm,
+         out_ref, next_hbm, tok_ref, small, *rest)
+
+
+def work(
+    nz,
+    share,
+    tok_hbm,
+    state_hbm,
+    w_hbm,
+    small_hbm,
+    eg_hbm,
+    eu_hbm,
+    ed_hbm,
+    out_ref,
+    next_hbm,
+    tok_ref,
+    small,
     st,
+    sn,
     wstage,
     wsend,
     wb,
@@ -82,6 +100,7 @@
     gh,
     ro,
     sv,
+    bh,
     eg,
     eu,
     ed,
@@ -111,8 +130,12 @@
     f1_recv,
     f2_send,
     f2_recv,
-    bar_wait_dummy,
+    small_sem,
 ):
+    (
+        dl1, dl2, doff, cl1, cl2, coff, gl1, gl2, blend,
+        sscale, hgain, hbias, mgain, mbias, egain, ebias, routes, rweight,
+    ) = small
     nk = nz // STRIDE
     dim = HEAD * nz
     half = dim // 2
@@ -149,7 +172,8 @@
             bar, inc=1, device_id={"grp": gbase + (gq + i) % share}, device_id_type=MESH
         )
 
-    w_hbm = (wr_hbm, wk_hbm, wv_hbm, wo_hbm)
+    tok_load = pltpu.make_async_copy(tok_hbm, tok_ref, ld_sem.at[8])
+    tok_load.start()
     for i in range(nm):
         for m in range(4):
             if m % nm == i:
@@ -162,6 +186,12 @@
     eg_load = pltpu.make_async_copy(eg_hbm.at[0], eg, ld_sem.at[5])
     eu_load = pltpu.make_async_copy(eu_hbm.at[0], eu, ld_sem.at[6])
     ed_load = pltpu.make_async_copy(ed_hbm.at[0], ed, ld_sem.at[7])
+    small_loads = [
+        pltpu.make_async_copy(a, b, small_sem.at[i])
+        for i, (a, b) in enumerate(zip(small_hbm, small))
+    ]
+    for cp in small_loads:
+        cp.start()
     st_load.start()
     eg_load.start()
     eu_load.start()
@@ -173,6 +203,7 @@
     lane16 = lane_ids((16, 128))
     left16 = lane16 < HEAD
 
+    tok_load.wait()
     tok = tok_ref[...].astype(F32)
     tok8[0:ROWS, :] = tok
     tok8[ROWS : 2 * ROWS, :] = tok
@@ -193,6 +224,8 @@
 
         wb[gq * nm + i, c, z] = wsend[i, z]
 
+    for cp in small_loads:
+        cp.wait()
     weight = rweight[...]
     part = weight / jnp.sum(weight, -1, keepdims=True)
     ids = routes[...]
@@ -209,85 +242,84 @@
     my_slot = slot_of(z)
     cb[c, my_slot] = csend[...]
 
-    def gather_start(buf, n):
-        for d in [nk // 2] + [x for y in range(nk // 2 - 1, 0, -1) for x in (y, nk - y)]:
-            kt = (own_k + d) % nk
-            pltpu.make_async_remote_copy(
-                src_ref=buf.at[res, own_k],
-                dst_ref=buf.at[res, own_k],
-                send_sem=l1_send.at[n, d],
-                recv_sem=l1_recv.at[n, nk - d],
-                device_id=chip(kt * STRIDE + res),
-                device_id_type=MESH,
-            ).start()
-
-    def level_two(buf, n):
-        hk = nk // 2
-        up, down, far = (res + 1) % STRIDE, (res + STRIDE - 1) % STRIDE, (res + 2) % STRIDE
-        steps = (
-            (1, buf.at[res], buf.at[down]),
-            (nz - 1, buf.at[res], buf.at[up]),
-            (2, buf.at[res, pl.ds(0, hk)], buf.at[far, pl.ds(0, hk)]),
-            (nz - 2, buf.at[res, pl.ds(hk, hk)], buf.at[far, pl.ds(hk, hk)]),
+    side = 1 - 2 * (own_k % 2)
+    hk = nk // 2
+
+    def step_copy(buf, n, slot, sem, kt):
+        at = buf.at[res, slot % nk]
+        return pltpu.make_async_remote_copy(
+            src_ref=at,
+            dst_ref=at,
+            send_sem=l1_send.at[n, sem],
+            recv_sem=l1_recv.at[n, sem],
+            device_id=chip((kt % nk) * STRIDE + res),
+            device_id_type=MESH,
         )
-        sends, recvs = [], []
-        for i, (d, src, arrives) in enumerate(steps):
-            sends.append(
-                pltpu.make_async_remote_copy(
-                    src_ref=src,
-                    dst_ref=src,
-                    send_sem=l2_send.at[n, i],
-                    recv_sem=l2_recv.at[n, i],
-                    device_id=chip(z + d),
-                    device_id_type=MESH,
-                )
-            )
-            recvs.append(
-                pltpu.make_async_remote_copy(
-                    src_ref=arrives,
-                    dst_ref=arrives,
-                    send_sem=l2_send.at[n, i],
-                    recv_sem=l2_recv.at[n, i],
-                    device_id=chip(z + d),
-                    device_id_type=MESH,
-                )
-            )
-        return sends, recvs
-
-    def gather_relay(buf, n):
-        for d in range(1, nk):
-            at = buf.at[res, (own_k + d) % nk]
+
+    def near_copies(buf, n, slot):
+        k = slot % nk
+        at = buf.at[res, k]
+        part = k // hk
+        for i, to, sem in ((0, z + 1, 0), (1, z + nz - 1, 1), (2, z + nz + 2 - 4 * part, 2 + part)):
             pltpu.make_async_remote_copy(
                 src_ref=at,
                 dst_ref=at,
-                send_sem=l1_send.at[n, d],
-                recv_sem=l1_recv.at[n, d],
-                device_id=chip(z),
+                send_sem=l2_send.at[n, i],
+                recv_sem=l2_recv.at[n, sem],
+                device_id=chip(to),
                 device_id_type=MESH,
-            ).wait_recv()
-        sends, _ = level_two(buf, n)
-        for s in sends:
-            s.start()
+            ).start()
+
+    direct = [(0, -1), (1, 1)] + ([(2, -2), (3, 2)] if nk > 4 else []) if nk > 2 else []
+    direct += [(6, nk // 2)] if nk in (2, 4) else []
+    onward = [(4, -3), (5, 3), (6, 4)] if nk == 8 else []
+
+    def gather_start(buf, n):
+        for sem, o in reversed(direct):
+            step_copy(buf, n, own_k, sem, own_k + nk - o).start()
+        near_copies(buf, n, own_k)
+
+    def gather_direct(buf, n):
+        for sem, o in direct:
+            step_copy(buf, n, own_k + nk + o, sem, own_k).wait_recv()
+            if sem == 2 and onward:
+                step_copy(buf, n, own_k + nk - 2, 4, own_k + 1).start()
+            if sem == 3 and onward:
+                step_copy(buf, n, own_k + nk + 2, 5, own_k + nk - 1).start()
+                step_copy(buf, n, own_k + nk - 2 * side, 6, own_k + nk + 2 * side).start()
+            if sem < 2 or not onward:
+                near_copies(buf, n, own_k + nk + o)
+        if onward:
+            near_copies(buf, n, own_k + nk - 2)
+            near_copies(buf, n, own_k + nk + 2)
+
+    def gather_onward(buf, n):
+        for sem, o in onward:
+            step_copy(buf, n, own_k + nk + o, sem, own_k).wait_recv()
+            near_copies(buf, n, own_k + nk + o)
+
+    def near_all(buf, n, i, sem, r, k0, count):
+        at = buf.at[r, pl.ds(k0, count)]
+        return pltpu.make_async_remote_copy(
+            src_ref=at,
+            dst_ref=at,
+            send_sem=l2_send.at[n, i],
+            recv_sem=l2_recv.at[n, sem],
+            device_id=chip(z + 1),
+            device_id_type=MESH,
+        )
 
     def gather_wait(buf, n):
-        _, recvs = level_two(buf, n)
-        for r in recvs:
-            r.wait_recv()
+        near_all(buf, n, 0, 0, (res + STRIDE - 1) % STRIDE, 0, nk).wait_recv()
+        near_all(buf, n, 1, 1, (res + 1) % STRIDE, 0, nk).wait_recv()
+        near_all(buf, n, 2, 2, (res + 2) % STRIDE, 0, hk).wait_recv()
+        near_all(buf, n, 2, 3, (res + 2) % STRIDE, hk, hk).wait_recv()
 
     def gather_drain(buf, n):
-        for d in range(1, nk):
-            at = buf.at[res, own_k]
-            pltpu.make_async_remote_copy(
-                src_ref=at,
-                dst_ref=at,
-                send_sem=l1_send.at[n, d],
-                recv_sem=l1_recv.at[n, d],
-                device_id=chip(z),
-                device_id_type=MESH,
-            ).wait_send()
-        sends, _ = level_two(buf, n)
-        for s in sends:
-            s.wait_send()
+        for sem, _ in direct + onward:
+            step_copy(buf, n, own_k, sem, own_k).wait_send()
+        for i in range(3):
+            near_all(buf, n, i, i, res, 0, nk).wait_send()
 
     def scatter(src_of, dst, send_sem, recv_sem):
         @pl.loop(0, nz - 1)
@@ -314,14 +346,18 @@
 
     pl.semaphore_wait(bar, nz - 1 + 1 + share - 1)
 
-    gather_start(xt, 0)
     for i in range(nm):
         m = gq * nm + i
         scatter(lambda zt, i=i: wsend.at[i, zt], wb.at[m, c, z], w_send.at[i], w_recv.at[i])
+    gather_start(xt, 0)
 
     tokb = tok8[...].astype(BF16)
-    squash = jnp.tanh(dot(tokb, dl1[...])).astype(BF16)
-    lowl = dot(tokb, cl1[...]).astype(BF16)
+
+    def dot_t(a, b):
+        return lax.dot_general(a, b, (((1,), (1,)), ((), ())), preferred_element_type=F32)
+
+    squash = jnp.tanh(dot_t(tokb, dl1[...])).astype(BF16)
+    lowl = dot_t(tokb, cl1[...]).astype(BF16)
     opened = jax.nn.sigmoid(dot(tokb, gl1[...])).astype(BF16)
 
     for j in range(nz // 2):
@@ -336,7 +372,7 @@
         two_heads(ah, jax.nn.sigmoid(coff[:, cols] + dot(lowl, cl2[:, cols])))
         two_heads(gh, dot(opened, gl2[:, cols]))
 
-    gather_relay(xt, 0)
+    gather_direct(xt, 0)
 
     def slab(m, core, to, send_sem, recv_sem):
         return pltpu.make_async_remote_copy(
@@ -360,6 +396,7 @@
                 q_recv.at[share - g, i],
             ).start()
         slab(m, c, sib, s_send.at[0, i], s_recv.at[0, i]).start()
+    gather_onward(xt, 0)
     for g in range(1, share):
         for i in range(nm):
             m = ((gq + g) % share) * nm + i
@@ -421,42 +458,48 @@
         tile = jnp.broadcast_to(ref[:, 128 * j : 128 * j + 128], (8, 128))
         return tile, pltpu.roll(tile, HEAD, 1)
 
-    blends, scales = [], []
+    blends = []
     for j in range(nz // 2):
         blends += pick(blend, j)
-        scales += pick(sscale, j)
     for h in range(nz):
-        ro[h] = blends[h]
-        sv[h] = scales[h]
-
-    @pl.loop(0, nz)
-    def _(h):
-        y = yrecv[h].astype(F32)
-        turned = pltpu.roll(y, ROWS, 0)
-        rk = jnp.where(top, y, turned)
-        v = jnp.where(top, turned, y)
-        r = jnp.where(left, rk, 0.0)
-        k = jnp.where(left, pltpu.roll(rk, HEAD, 1), 0.0)
-        a = ah[h]
-        unit = k * lax.rsqrt(jnp.sum(k * k, -1, keepdims=True) + 1e-06)
-        written = k * (1.0 + (a - 1.0) * ro[h])
-        ua = unit * a
-        own = jnp.sum(r * written * sv[h], -1, keepdims=True)
-        d = dh[h]
-        sv[h] = own * v
-        for t in range(ROWS):
-            one = slice(t, t + 1)
-            s = st[t, h]
-            removed = jnp.sum(s * unit[one, 0:HEAD], -1, keepdims=True)
-            vcol = jnp.sum(eye * v[one, 0:HEAD], -1, keepdims=True)
-            n = s * d[one, 0:HEAD] - removed * ua[one, 0:HEAD] + vcol * written[one, 0:HEAD]
-            st[t, h] = n
-            rcol = jnp.sum(n * r[one, 0:HEAD], -1, keepdims=True)
-            row = jnp.sum(eye * rcol, 0, keepdims=True)
-            ro[h, t : t + 1, 0:HEAD] = row
-            ro[h, ROWS + t : ROWS + t + 1, 0:HEAD] = row
-
-    st_store = pltpu.make_async_copy(st, next_hbm, ld_sem.at[4])
+        bh[h] = blends[h]
+
+    ones = jnp.ones((HEAD, HEAD), BF16)
+
+    def row_sums(x):
+        high = x.astype(BF16)
+        low = (x - high.astype(F32)).astype(BF16)
+        return dot(high, ones) + dot(low, ones)
+
+    @pl.loop(0, nz // 2)
+    def _(pair):
+        for h in (2 * pair, 2 * pair + 1):
+            y = yrecv[h].astype(F32)
+            turned = pltpu.roll(y, ROWS, 0)
+            rk = jnp.where(top, y, turned)
+            v = jnp.where(top, turned, y)
+            r = jnp.where(left, rk, 0.0)
+            k = jnp.where(left, pltpu.roll(rk, HEAD, 1), 0.0)
+            a = ah[h]
+            unit = k * lax.rsqrt(jnp.sum(k * k, -1, keepdims=True) + 1e-06)
+            written = k * (1.0 + (a - 1.0) * bh[h])
+            ua = unit * a
+            scale = sscale[pl.ds(h, 1), :]
+            own = jnp.sum((r * written)[:, 0:HEAD] * scale, -1, keepdims=True)
+            d = dh[h]
+            sv[h] = own * v
+            for t in range(ROWS):
+                one = slice(t, t + 1)
+                s = st[t, h]
+                removed = row_sums(s * unit[one, 0:HEAD])
+                vcol = dot((eye * v[one, 0:HEAD]).astype(BF16), ones)
+                n = s * d[one, 0:HEAD] - removed * ua[one, 0:HEAD] + vcol * written[one, 0:HEAD]
+                sn[t, h] = n
+                row = jnp.sum(eye * row_sums(n * r[one, 0:HEAD]), 0, keepdims=True)
+                ro[h, t : t + 1, 0:HEAD] = row
+                ro[h, ROWS + t : ROWS + t + 1, 0:HEAD] = row
+
+    st_store = pltpu.make_async_copy(sn, next_hbm, ld_sem.at[4])
     st_store.start()
 
     def mixer_head(h, gain, bias):
@@ -478,7 +521,8 @@
         xm[res, own_k, :, 128 * j : 128 * j + 128] = tile.astype(BF16)
 
     gather_start(xm, 1)
-    gather_relay(xm, 1)
+    gather_direct(xm, 1)
+    gather_onward(xm, 1)
     gather_wait(xm, 1)
     co = fold(dot(rows_of(xm[...]), em[:, 768:1024]))
     co_high = co.astype(BF16).astype(F32)
@@ -531,7 +575,8 @@
     xh[c, res, own_k] = hidden
     mine = xh.at[c]
     gather_start(mine, 2)
-    gather_relay(mine, 2)
+    gather_direct(mine, 2)
+    gather_onward(mine, 2)
     gather_wait(mine, 2)
     to_sib(xh.at[c], xh.at[c], 1).start()
 
@@ -575,61 +620,85 @@
     to_sib(zoth, zsib, 2).wait_recv()
     tsum[...] = (zown[...].astype(F32) + zsib[...].astype(F32)).astype(BF16)
 
-    hk = nk // 2
-    up, down_, far = (res + 1) % STRIDE, (res + STRIDE - 1) % STRIDE, (res + 2) % STRIDE
-    first = (
-        (1, tsum.at[up], r1.at[0]),
-        (nz - 1, tsum.at[down_], r1.at[1]),
-        (2, tsum.at[far, pl.ds(0, hk)], r1.at[2, pl.ds(0, hk)]),
-        (nz - 2, tsum.at[far, pl.ds(hk, hk)], r1.at[2, pl.ds(hk, hk)]),
-    )
-    copies = [
-        pltpu.make_async_remote_copy(
-            src_ref=src,
-            dst_ref=dst,
-            send_sem=f1_send.at[i],
-            recv_sem=f1_recv.at[i],
-            device_id=chip(z + d),
+    def near_sum(slot):
+        k = slot % nk
+        part = k // hk
+        up, down_, far = (res + 1) % STRIDE, (res + STRIDE - 1) % STRIDE, (res + 2) % STRIDE
+        return [
+            pltpu.make_async_remote_copy(
+                src_ref=tsum.at[r, k],
+                dst_ref=r1.at[i, k],
+                send_sem=f1_send.at[i],
+                recv_sem=f1_recv.at[i, k],
+                device_id=chip(to),
+                device_id_type=MESH,
+            )
+            for i, (to, r) in enumerate(
+                ((z + 1, up), (z + nz - 1, down_), (z + nz + 2 - 4 * part, far))
+            )
+        ]
+
+    def step_sum(kt, src, sem):
+        return pltpu.make_async_remote_copy(
+            src_ref=u2.at[src],
+            dst_ref=r2.at[sem],
+            send_sem=f2_send.at[sem],
+            recv_sem=f2_recv.at[sem],
+            device_id=chip((kt % nk) * STRIDE + res),
             device_id_type=MESH,
         )
-        for i, (d, src, dst) in enumerate(first)
-    ]
-    for cp in copies:
-        cp.start()
-    for cp in copies:
-        cp.wait_recv()
-    u2[...] = (
-        tsum[res].astype(F32)
-        + r1[0].astype(F32)
-        + r1[1].astype(F32)
-        + r1[2].astype(F32)
-    ).astype(BF16)
-
-    def last(d):
-        kt = (own_k + d) % nk
-        return pltpu.make_async_remote_copy(
-            src_ref=u2.at[kt],
-            dst_ref=r2.at[nk - d],
-            send_sem=f2_send.at[d],
-            recv_sem=f2_recv.at[nk - d],
-            device_id=chip(kt * STRIDE + res),
-            device_id_type=MESH,
+
+    def near_total(slot):
+        k = slot % nk
+        for cp in near_sum(k):
+            cp.wait_recv()
+        return (
+            tsum[res, k].astype(F32)
+            + r1[0, k].astype(F32)
+            + r1[1, k].astype(F32)
+            + r1[2, k].astype(F32)
         )
 
-    for d in [nk // 2] + [x for y in range(nk // 2 - 1, 0, -1) for x in (y, nk - y)]:
-        last(d).start()
-    total = hidp[...] + u2[own_k].astype(F32)
-    for d in range(1, nk):
-        pltpu.make_async_remote_copy(
-            src_ref=r2.at[d],
-            dst_ref=r2.at[d],
-            send_sem=f2_send.at[d],
-            recv_sem=f2_recv.at[d],
-            device_id=chip(z),
-            device_id_type=MESH,
-        ).wait_recv()
-    for d in range(1, nk):
-        total = total + r2[d].astype(F32)
+    def arrived(sem):
+        step_sum(own_k, 0, sem).wait_recv()
+        return r2[sem].astype(F32)
+
+    if nk == 8:
+        order = [nk + 4, nk - 3, nk + 3, nk - 2 * side, nk + 2 * side, nk - 1, nk + 1, nk]
+    else:
+        order = [nk // 2] + ([1, nk - 1] if nk == 4 else []) + [nk]
+    for o in order:
+        for cp in near_sum(own_k + o):
+            cp.start()
+    if nk == 8:
+        u2[0] = near_total(own_k + 4).astype(BF16)
+        step_sum(own_k + nk + 2 * side * -1, 0, 0).start()
+        u2[1] = near_total(own_k + nk - 3 * side).astype(BF16)
+        step_sum(own_k + nk - side, 1, 1).start()
+        u2[2] = near_total(own_k + nk + 3 * side).astype(BF16)
+        step_sum(own_k + nk + side, 2, 2).start()
+        u2[3] = near_total(own_k + nk - side).astype(BF16)
+        step_sum(own_k + nk - side, 3, 3).start()
+        u2[4] = near_total(own_k + nk + side).astype(BF16)
+        step_sum(own_k + nk + side, 4, 4).start()
+        part_b = near_total(own_k + nk + 2 * side)
+        part_a = near_total(own_k + nk - 2 * side)
+        u2[6] = (part_b + arrived(1)).astype(BF16)
+        step_sum(own_k + nk + 2 * side, 6, 6).start()
+        u2[5] = (part_a + arrived(2) + arrived(0)).astype(BF16)
+        step_sum(own_k + nk - 2 * side, 5, 5).start()
+        total = near_total(own_k)
+        used = range(7)
+    else:
+        for i, o in enumerate(order[:-1]):
+            u2[i] = near_total(own_k + o).astype(BF16)
+            step_sum(own_k + o, i, i).start()
+        total = near_total(own_k)
+        used = range(len(order) - 1)
+    total = total + hidp[...]
+    for sem in used:
+        if nk != 8 or sem >= 3:
+            total = total + arrived(sem)
     y = layer_norm(total, egain, ebias)
     out_ref[:, 0:half] = y[0:ROWS, :].astype(BF16)
     out_ref[:, half:dim] = y[ROWS : 2 * ROWS, :].astype(BF16)
@@ -650,10 +719,17 @@
     to_sib(cb.at[c], cb.at[c], 0).wait_send()
     to_sib(xh.at[c], xh.at[c], 1).wait_send()
     to_sib(zoth, zsib, 2).wait_send()
-    for cp in copies:
-        cp.wait_send()
-    for d in range(1, nk):
-        last(d).wait_send()
+    for i in range(3):
+        pltpu.make_async_remote_copy(
+            src_ref=tsum.at[res],
+            dst_ref=r1.at[i],
+            send_sem=f1_send.at[i],
+            recv_sem=f1_recv.at[i, 0],
+            device_id=chip(z + 1),
+            device_id_type=MESH,
+        ).wait_send()
+    for sem in used:
+        step_sum(own_k, sem, sem).wait_send()
     st_store.wait()
 
 
@@ -665,18 +741,20 @@
     nm = 4 // share
     ff = args[24].shape[2]
     args = list(args)
-    for i in (7, 10, 13, 14, 15, 16, 18, 19, 20, 21):
+    args[5], args[8] = args[5].T, args[8].T
+    for i in (7, 10, 13, 15, 16, 18, 19, 20, 21):
         args[i] = args[i].reshape(1, dim)
-    order = [0, 1, 2, 3, 4, 17, 5, 6, 7, 8, 9, 10, 11, 12, 13, 14, 15, 16, 18, 19, 20, 21]
-    order += [22, 23, 24, 25, 26]
-    operands = [args[i] for i in order]
-    in_hbm = {1, 2, 3, 4, 5, 24, 25, 26}
+    small = [5, 6, 7, 8, 9, 10, 11, 12, 13, 14, 15, 16, 18, 19, 20, 21, 22, 23]
+    operands = [args[i] for i in [0, 1, 2, 3, 4, 17] + small + [24, 25, 26]]
     vmem = pl.BlockSpec(memory_space=pltpu.VMEM)
     hbm = pl.BlockSpec(memory_space=pl.ANY)
     dma = pltpu.SemaphoreType.DMA
     heads = (nz, 8, 128)
     rows = (STRIDE, nk, 8, half)
     scratch = [
+        pltpu.VMEM(tokens.shape, BF16),
+        *[pltpu.VMEM(args[i].shape, args[i].dtype) for i in small],
+        pltpu.VMEM(state.shape, F32),
         pltpu.VMEM(state.shape, F32),
         pltpu.VMEM((nm, 32, dim), BF16),
         pltpu.VMEM((nm, nz, 16, 128), BF16),
@@ -699,6 +777,7 @@
         pltpu.VMEM(heads, F32),
         pltpu.VMEM(heads, F32),
         pltpu.VMEM(heads, F32),
+        pltpu.VMEM(heads, F32),
         pltpu.VMEM((dim, ff), BF16),
         pltpu.VMEM((dim, ff), BF16),
         pltpu.VMEM((ff, dim), BF16),
@@ -709,34 +788,34 @@
         pltpu.VMEM((3, nk, 8, half), BF16),
         pltpu.VMEM((nk, 8, half), BF16),
         pltpu.VMEM((nk, 8, half), BF16),
-        dma((8,)),
+        dma((9,)),
         dma((nm,)),
         dma((nm,)),
         dma((share, nm)),
         dma((share, nm)),
         dma((share, nm)),
         dma((share, nm)),
-        dma((3, nk)),
-        dma((3, nk)),
-        dma((3, 4)),
+        dma((3, 7)),
+        dma((3, 7)),
+        dma((3, 3)),
         dma((3, 4)),
         dma((3,)),
         dma((3,)),
         dma((3,)),
         dma((3,)),
-        dma((4,)),
-        dma((4,)),
-        dma((nk,)),
-        dma((nk,)),
-        dma((1,)),
+        dma((3,)),
+        dma((3, nk)),
+        dma((7,)),
+        dma((7,)),
+        dma((SMALL,)),
     ]
     return pl.pallas_call(
-        functools.partial(kernel, nz, share, ff),
+        functools.partial(kernel, nz, share),
         out_shape=(
             jax.ShapeDtypeStruct(tokens.shape, BF16),
             jax.ShapeDtypeStruct(state.shape, F32),
         ),
-        in_specs=[hbm if i in in_hbm else vmem for i in range(len(operands))],
+        in_specs=[hbm] * len(operands),
         out_specs=(vmem, hbm),
         scratch_shapes=scratch,
         compiler_params=pltpu.CompilerParams(

time: 204 us -> 194 us (0.951)
  local copies, waits for them, and re-layouts: 11.4 us -> 6.12 us
  Pallas kernels: 189 us -> 186 us
    unnamed x4 -> x2, local copies, waits for them, and re-layouts: 10 us -> 6.12 us
    pallas_call x1, Pallas kernels: 189 us -> 186 us  [step(): pl.pallas_call(functools.partial(kernel, nz, share), out_shape=(jax.Shape...]
where the time goes in v2:
time: 194 us; the launch traced here: 192 us
  Pallas kernels  186 us (96%)
  local copies, waits for them, and re-layouts  6.12 us (3%)
    pallas_call x1, Pallas kernels, step(): pl.pallas_call(functools.partial(kernel, nz, share), out_shape=(jax.Shape...  186 us
    unnamed x2, local copies, waits for them, and re-layouts  6.12 us

profile of v2, /device:TPU:46, one launch (start us, length us, event | category | flops | bytes accessed | tf_op | source)
XLA Modules:
  0.0 192.3 jit_solution(15923049187138736440)
XLA Ops:
  0.6 185.5 %shard_map.266 = (bf16[4,2048]{1,0:T(4,128)(2,1)}, f32[4,32,64,64]{3,2,1,0:T(8,128)}) custom-call(bf16[4,2048]{1,0:T(4,128)(2,1)} %tok_hbm.1, f32[4,32,64,64]{3,2,1,0:T(8,128)} %state_hbm.1, bf16[32,2048]{1,0:T(8,128)(2,1)} %wr_hbm.1, bf16[32,2048]{1,0:T(8,128)(2,1)} %wk_hbm.1, bf16[32,2048]{1,0:T(8,128)(2,1)} %wv_hbm.1, bf16[32,2048]{1,0:T(8,128)(2,1)} %wo_hbm.1, ...), custom_call_target="tpu_custom_call" | custom-call | tf_op jit(solution)/shard_map/pallas_call | solution.py:812
  186.2 1.3 copy.31
  187.5 4.8 %copy.32 = f32[4,32,64,64]{3,2,1,0:T(8,128)} copy(f32[4,32,64,64]{3,2,1,0:T(8,128)} %get-tuple-element.5) | data formatting | bytes 4194304

commit v3 on v2

--- a/solution.py
+++ b/solution.py
@@ -344,33 +344,33 @@
             device_id_type=MESH,
         )
 
+    tokb = tok8[...].astype(BF16)
+
+    def dot_t(a, b):
+        return lax.dot_general(a, b, (((1,), (1,)), ((), ())), preferred_element_type=F32)
+
+    squash = jnp.tanh(dot_t(tokb, dl1[...])).astype(BF16)
+    lowl = dot_t(tokb, cl1[...]).astype(BF16)
+    opened = jax.nn.sigmoid(dot(tokb, gl1[...])).astype(BF16)
+
+    for j in range(nz // 2):
+        cols = slice(128 * j, 128 * j + 128)
+
+        def two_heads(ref, tile, j=j):
+            ref[2 * j] = tile
+            ref[2 * j + 1] = pltpu.roll(tile, HEAD, 1)
+
+        pre = doff[:, cols] + dot(squash, dl2[:, cols])
+        two_heads(dh, jnp.exp(-(jnp.exp(jnp.full((8, 128), -0.5, F32)) * jax.nn.sigmoid(pre))))
+        two_heads(ah, jax.nn.sigmoid(coff[:, cols] + dot(lowl, cl2[:, cols])))
+        two_heads(gh, dot(opened, gl2[:, cols]))
+
     pl.semaphore_wait(bar, nz - 1 + 1 + share - 1)
 
     for i in range(nm):
         m = gq * nm + i
         scatter(lambda zt, i=i: wsend.at[i, zt], wb.at[m, c, z], w_send.at[i], w_recv.at[i])
     gather_start(xt, 0)
-
-    tokb = tok8[...].astype(BF16)
-
-    def dot_t(a, b):
-        return lax.dot_general(a, b, (((1,), (1,)), ((), ())), preferred_element_type=F32)
-
-    squash = jnp.tanh(dot_t(tokb, dl1[...])).astype(BF16)
-    lowl = dot_t(tokb, cl1[...]).astype(BF16)
-    opened = jax.nn.sigmoid(dot(tokb, gl1[...])).astype(BF16)
-
-    for j in range(nz // 2):
-        cols = slice(128 * j, 128 * j + 128)
-
-        def two_heads(ref, tile, j=j):
-            ref[2 * j] = tile
-            ref[2 * j + 1] = pltpu.roll(tile, HEAD, 1)
-
-        pre = doff[:, cols] + dot(squash, dl2[:, cols])
-        two_heads(dh, jnp.exp(-(jnp.exp(jnp.full((8, 128), -0.5, F32)) * jax.nn.sigmoid(pre))))
-        two_heads(ah, jax.nn.sigmoid(coff[:, cols] + dot(lowl, cl2[:, cols])))
-        two_heads(gh, dot(opened, gl2[:, cols]))
 
     gather_direct(xt, 0)
 
@@ -463,13 +463,6 @@
         blends += pick(blend, j)
     for h in range(nz):
         bh[h] = blends[h]
-
-    ones = jnp.ones((HEAD, HEAD), BF16)
-
-    def row_sums(x):
-        high = x.astype(BF16)
-        low = (x - high.astype(F32)).astype(BF16)
-        return dot(high, ones) + dot(low, ones)
 
     @pl.loop(0, nz // 2)
     def _(pair):
@@ -491,11 +484,12 @@
             for t in range(ROWS):
                 one = slice(t, t + 1)
                 s = st[t, h]
-                removed = row_sums(s * unit[one, 0:HEAD])
-                vcol = dot((eye * v[one, 0:HEAD]).astype(BF16), ones)
+                removed = jnp.sum(s * unit[one, 0:HEAD], -1, keepdims=True)
+                vcol = jnp.sum(eye * v[one, 0:HEAD], -1, keepdims=True)
                 n = s * d[one, 0:HEAD] - removed * ua[one, 0:HEAD] + vcol * written[one, 0:HEAD]
                 sn[t, h] = n
-                row = jnp.sum(eye * row_sums(n * r[one, 0:HEAD]), 0, keepdims=True)
+                read = jnp.sum(n * r[one, 0:HEAD], -1, keepdims=True)
+                row = jnp.sum(eye * read, 0, keepdims=True)
                 ro[h, t : t + 1, 0:HEAD] = row
                 ro[h, ROWS + t : ROWS + t + 1, 0:HEAD] = row
 

time: 194 us -> 177 us (0.912)
  Pallas kernels: 186 us -> 170 us
    pallas_call x1, Pallas kernels: 186 us -> 170 us  [step(): pl.pallas_call(functools.partial(kernel, nz, share), out_shape=(jax.Shape...]
where the time goes in v3:
time: 177 us
  Pallas kernels  170 us (96%)
  local copies, waits for them, and re-layouts  6.12 us (3%)
    pallas_call x1, Pallas kernels, step(): pl.pallas_call(functools.partial(kernel, nz, share), out_shape=(jax.Shape...  170 us
    unnamed x2, local copies, waits for them, and re-layouts  6.12 us

profile of v3, /device:TPU:46, one launch (start us, length us, event | category | flops | bytes accessed | tf_op | source)
XLA Modules:
  0.0 176.9 jit_solution(11461181727658437037)
XLA Ops:
  0.6 170.2 %shard_map.266 = (bf16[4,2048]{1,0:T(4,128)(2,1)}, f32[4,32,64,64]{3,2,1,0:T(8,128)}) custom-call(bf16[4,2048]{1,0:T(4,128)(2,1)} %tok_hbm.1, f32[4,32,64,64]{3,2,1,0:T(8,128)} %state_hbm.1, bf16[32,2048]{1,0:T(8,128)(2,1)} %wr_hbm.1, bf16[32,2048]{1,0:T(8,128)(2,1)} %wk_hbm.1, bf16[32,2048]{1,0:T(8,128)(2,1)} %wv_hbm.1, bf16[32,2048]{1,0:T(8,128)(2,1)} %wo_hbm.1, ...), custom_call_target="tpu_custom_call" | custom-call | tf_op jit(solution)/shard_map/pallas_call | solution.py:806
  170.8 1.3 copy.31
  172.1 4.8 %copy.32 = f32[4,32,64,64]{3,2,1,0:T(8,128)} copy(f32[4,32,64,64]{3,2,1,0:T(8,128)} %get-tuple-element.5) | data formatting | bytes 4194304

commit v4 on v3

--- a/solution.py
+++ b/solution.py
@@ -85,11 +85,11 @@
     em,
     xt,
     xm,
-    xh,
+    xg,
+    x2,
+    hid,
     ysend,
     yrecv,
-    msend,
-    mrecv,
     cb,
     csend,
     tok8,
@@ -446,6 +446,16 @@
     scatter(lambda zt: ysend.at[slot_of(zt)], yrecv.at[z], a_send.at[0], a_recv.at[0])
     yrecv[z] = ysend[my_slot]
     scatter(lambda zt: csend, cb.at[c, my_slot], a_send.at[2], a_recv.at[2])
+    topk = row_ids((nk, 8, 128)) < ROWS
+    leftk = lane_ids((nk, 8, 128)) < HEAD
+    for s in range(2):
+        for m in range(half // 128):
+            one = xt[2 * s, :, :, 128 * m : 128 * m + 128].astype(F32)
+            two = xt[2 * s + 1, :, :, 128 * m : 128 * m + 128].astype(F32)
+            x2[s, :, :, 128 * m : 128 * m + 128] = jnp.where(topk, one, pltpu.roll(two, ROWS, 1))
+            x2[s, :, :, half + 128 * m : half + 128 * m + 128] = jnp.where(
+                topk, pltpu.roll(one, ROWS, 1), two
+            )
     st_load.wait()
     scatter_all(yrecv, a_send.at[0], a_recv.at[0]).wait_recv()
 
@@ -519,10 +529,12 @@
     gather_onward(xm, 1)
     gather_wait(xm, 1)
     co = fold(dot(rows_of(xm[...]), em[:, 768:1024]))
-    co_high = co.astype(BF16).astype(F32)
-    msend[...] = jnp.where(top3, co_high, co - co_high).astype(BF16)
-    scatter(lambda zt: msend.at[slot_of(zt)], mrecv.at[z], a_send.at[1], a_recv.at[1])
-    mrecv[z] = msend[my_slot]
+    xg[res, own_k] = jnp.where(
+        leftk,
+        jnp.where(topk, co[0:nk], co[nk : 2 * nk]),
+        jnp.where(topk, co[2 * nk : 3 * nk], co[3 * nk :]),
+    ).astype(BF16)
+    gather_start(xg, 2)
 
     scatter_all(cb.at[c], a_send.at[2], a_recv.at[2]).wait_recv()
 
@@ -538,16 +550,28 @@
 
     to_sib(cb.at[c], cb.at[c], 0).start()
 
-    scatter_all(mrecv, a_send.at[1], a_recv.at[1]).wait_recv()
-    for j in range(nz // 4):
-
-        def mixed_pair(p):
-            one, two = mrecv[2 * p].astype(F32), mrecv[2 * p + 1].astype(F32)
-            tile = jnp.where(left, one, two)
-            return tile + pltpu.roll(tile, ROWS, 0)
-
+    gather_direct(xg, 2)
+    gather_onward(xg, 2)
+    gather_wait(xg, 2)
+    for j in range(nz // 2):
         cols = slice(128 * j, 128 * j + 128)
-        tokp[:, cols] += jnp.where(top, mixed_pair(j), mixed_pair(nz // 4 + j))
+        one = xg[2 * j % STRIDE, 2 * j // STRIDE].astype(F32)
+        two = xg[(2 * j + 1) % STRIDE, (2 * j + 1) // STRIDE].astype(F32)
+        x2[0, :, :, cols] += jnp.where(leftk, one, pltpu.roll(two, HEAD, 2))
+        x2[1, :, :, cols] += jnp.where(leftk, pltpu.roll(one, HEAD, 2), two)
+
+    some = max(1, nk // 2)
+    for s in range(2):
+        for k in range(0, nk, some):
+            x = x2[s, k : k + some]
+            dev = x - jnp.mean(x, -1, keepdims=True)
+            var = jnp.mean(dev * dev, -1, keepdims=True)
+            y = dev * lax.rsqrt(var + 1e-05) * mgain[...] + mbias[...]
+            x2[s, k : k + some] = y
+            base = 8 * (s * nk + k)
+            hid[c, base : base + 8 * some, :] = y.reshape(8 * some, dim).astype(BF16)
+
+    to_sib(hid.at[c], hid.at[c], 1).start()
 
     topp = row_ids((8, half)) < ROWS
 
@@ -564,52 +588,54 @@
         var = row_total(dev * dev)
         return dev * lax.rsqrt(var + 1e-05) * packed(gain) + packed(bias)
 
-    hidden = layer_norm(tokp[...], mgain, mbias).astype(BF16)
-    hidp[...] = hidden.astype(F32)
-    xh[c, res, own_k] = hidden
-    mine = xh.at[c]
-    gather_start(mine, 2)
-    gather_direct(mine, 2)
-    gather_onward(mine, 2)
-    gather_wait(mine, 2)
-    to_sib(xh.at[c], xh.at[c], 1).start()
+    two_rows = x2[res // 2, own_k].astype(BF16).astype(F32)
+    mine = row_ids((8, dim)) // ROWS == res % 2
+    doubled = jnp.where(mine, two_rows, pltpu.roll(two_rows, ROWS, 0))
+    hidp[...] = jnp.where(topp, doubled[:, 0:half], doubled[:, half:dim])
 
     eg_load.wait()
     eu_load.wait()
     ed_load.wait()
     to_sib(cb.at[1 - c], cb.at[1 - c], 0).wait_recv()
 
-    def wide_fold(a, b):
-        width = a.shape[1]
-        keep = (row_ids((8 * nz, width)) % 8) < ROWS
-        x = jnp.where(keep, a, b).reshape(nz, 8, width)
-        return (x + pltpu.roll(x, ROWS, 1)).reshape(8 * nz, width)
-
     def expert(core):
-        xv = rows_of(xh[core])
+        xv = hid[core]
         lane3 = lane_ids((nz, 8, 128))
         hit = (lane3 == ep) | (lane3 == ep + HEAD)
         coef = jnp.sum(jnp.where(hit, cb[core].astype(F32), 0.0), -1, keepdims=True)
-        coef = coef.reshape(8 * nz, 1)
-        gate = wide_fold(dot(xv, eg[0:half, :]), dot(xv, eg[half:dim, :]))
-        up = wide_fold(dot(xv, eu[0:half, :]), dot(xv, eu[half:dim, :]))
+        top1 = row_ids((nk, 8, 1)) < ROWS
+        coef = jnp.concatenate(
+            [
+                jnp.where(top1, coef[0:nk], coef[nk : 2 * nk]),
+                jnp.where(top1, coef[2 * nk : 3 * nk], coef[3 * nk :]),
+            ],
+            0,
+        ).reshape(ROWS * nz, 1)
+        gate = dot(xv, eg[...])
+        up = dot(xv, eu[...])
         inner = (gate * jax.nn.sigmoid(gate) * up).astype(BF16)
         return inner, coef
 
-    def down(inner, coef, j, width):
-        a = dot(inner, ed[:, j * width : (j + 1) * width])
-        b = dot(inner, ed[:, half + j * width : half + (j + 1) * width])
-        keep = (row_ids((8 * nz, width)) % 8) < ROWS
-        return (jnp.where(keep, a, b) * coef).reshape(STRIDE, nk, 8, width)
+    def down(inner, coef, z, j, width):
+        cols = slice(j * width, (j + 1) * width)
+        low = dot(inner, ed[:, cols]) * coef
+        high = dot(inner, ed[:, half + j * width : half + (j + 1) * width]) * coef
+        low, high = low.reshape(2, nk, 8, width), high.reshape(2, nk, 8, width)
+        keep = row_ids((nk, 8, width)) < ROWS
+        for s in range(2):
+            one = jnp.where(keep, low[s], pltpu.roll(high[s], ROWS, 1))
+            two = jnp.where(keep, pltpu.roll(low[s], ROWS, 1), high[s])
+            z[2 * s, :, :, cols] = one.astype(BF16)
+            z[2 * s + 1, :, :, cols] = two.astype(BF16)
 
     width = min(256, half)
     inner, coef = expert(c)
     for j in range(half // width):
-        zown[:, :, :, j * width : (j + 1) * width] = down(inner, coef, j, width).astype(BF16)
-    to_sib(xh.at[1 - c], xh.at[1 - c], 1).wait_recv()
+        down(inner, coef, zown, j, width)
+    to_sib(hid.at[1 - c], hid.at[1 - c], 1).wait_recv()
     inner, coef = expert(1 - c)
     for j in range(half // width):
-        zoth[:, :, :, j * width : (j + 1) * width] = down(inner, coef, j, width).astype(BF16)
+        down(inner, coef, zoth, j, width)
     to_sib(zoth, zsib, 2).start()
     to_sib(zoth, zsib, 2).wait_recv()
     tsum[...] = (zown[...].astype(F32) + zsib[...].astype(F32)).astype(BF16)
@@ -699,7 +725,7 @@
 
     gather_drain(xt, 0)
     gather_drain(xm, 1)
-    gather_drain(mine, 2)
+    gather_drain(xg, 2)
     for i in range(nm):
         scatter_all(wb.at[gq * nm + i, c], w_send.at[i], w_recv.at[i]).wait_send()
         slab(gq * nm + i, c, sib, s_send.at[0, i], s_recv.at[0, i]).wait_send()
@@ -708,10 +734,9 @@
             m = ((gq + g) % share) * nm + i
             slab(m, c, sib, s_send.at[g, i], s_recv.at[g, i]).wait_send()
     scatter_all(yrecv, a_send.at[0], a_recv.at[0]).wait_send()
-    scatter_all(mrecv, a_send.at[1], a_recv.at[1]).wait_send()
     scatter_all(cb.at[c], a_send.at[2], a_recv.at[2]).wait_send()
     to_sib(cb.at[c], cb.at[c], 0).wait_send()
-    to_sib(xh.at[c], xh.at[c], 1).wait_send()
+    to_sib(hid.at[c], hid.at[c], 1).wait_send()
     to_sib(zoth, zsib, 2).wait_send()
     for i in range(3):
         pltpu.make_async_remote_copy(
@@ -756,9 +781,9 @@
         pltpu.VMEM((half, 1024), BF16),
         pltpu.VMEM(rows, BF16),
         pltpu.VMEM(rows, BF16),
-        pltpu.VMEM((2,) + rows, BF16),
-        pltpu.VMEM(heads, BF16),
-        pltpu.VMEM(heads, BF16),
+        pltpu.VMEM((STRIDE, nk, nk, 8, 128), BF16),
+        pltpu.VMEM((2, nk, 8, dim), F32),
+        pltpu.VMEM((2, ROWS * nz, dim), BF16),
         pltpu.VMEM(heads, BF16),
         pltpu.VMEM(heads, BF16),
         pltpu.VMEM((2,) + heads, BF16),

time: 177 us -> 163 us (0.921)
  Pallas kernels: 170 us -> 156 us
    pallas_call x1, Pallas kernels: 170 us -> 156 us  [step(): pl.pallas_call(functools.partial(kernel, nz, share), out_shape=(jax.Shape...]
where the time goes in v4:
time: 163 us
  Pallas kernels  156 us (96%)
  local copies, waits for them, and re-layouts  6.12 us (4%)
    pallas_call x1, Pallas kernels, step(): pl.pallas_call(functools.partial(kernel, nz, share), out_shape=(jax.Shape...  156 us
    unnamed x2, local copies, waits for them, and re-layouts  6.12 us

profile of v4, /device:TPU:46, one launch (start us, length us, event | category | flops | bytes accessed | tf_op | source)
XLA Modules:
  0.0 162.8 jit_solution(15646443269536323693)
XLA Ops:
  0.6 156.1 %shard_map.266 = (bf16[4,2048]{1,0:T(4,128)(2,1)}, f32[4,32,64,64]{3,2,1,0:T(8,128)}) custom-call(bf16[4,2048]{1,0:T(4,128)(2,1)} %tok_hbm.1, f32[4,32,64,64]{3,2,1,0:T(8,128)} %state_hbm.1, bf16[32,2048]{1,0:T(8,128)(2,1)} %wr_hbm.1, bf16[32,2048]{1,0:T(8,128)(2,1)} %wk_hbm.1, bf16[32,2048]{1,0:T(8,128)(2,1)} %wv_hbm.1, bf16[32,2048]{1,0:T(8,128)(2,1)} %wo_hbm.1, ...), custom_call_target="tpu_custom_call" | custom-call | tf_op jit(solution)/shard_map/pallas_call | solution.py:831
  156.7 1.3 copy.31
  158.0 4.8 %copy.32 = f32[4,32,64,64]{3,2,1,0:T(8,128)} copy(f32[4,32,64,64]{3,2,1,0:T(8,128)} %get-tuple-element.5) | data formatting | bytes 4194304

commit v5 on v4

--- a/solution.py
+++ b/solution.py
@@ -140,6 +140,7 @@
     dim = HEAD * nz
     half = dim // 2
     nm = 4 // share
+    quarter = nz // 4
     ep = lax.axis_index("ep")
     grp = lax.axis_index("grp")
     z = ep // 2
@@ -369,39 +370,65 @@
 
     for i in range(nm):
         m = gq * nm + i
-        scatter(lambda zt, i=i: wsend.at[i, zt], wb.at[m, c, z], w_send.at[i], w_recv.at[i])
+        scatter(
+            lambda zt, i=i: wsend.at[i, zt],
+            wb.at[m, c, z],
+            w_send.at[i],
+            w_recv.at[i, z // quarter],
+        )
     gather_start(xt, 0)
 
     gather_direct(xt, 0)
 
-    def slab(m, core, to, send_sem, recv_sem):
+    def piece(m, core, n, to, send_sem, recv_sem):
+        at = wb.at[m, core, pl.ds(n * quarter, quarter)]
         return pltpu.make_async_remote_copy(
-            src_ref=wb.at[m, core],
-            dst_ref=wb.at[m, core],
+            src_ref=at,
+            dst_ref=at,
             send_sem=send_sem,
             recv_sem=recv_sem,
             device_id=to,
             device_id_type=MESH,
         )
 
-    for i in range(nm):
-        m = gq * nm + i
-        scatter_all(wb.at[m, c], w_send.at[i], w_recv.at[i]).wait_recv()
-        for g in range(1, share):
-            slab(
-                m,
-                c,
-                {"grp": gbase + (gq + g) % share},
-                q_send.at[g, i],
-                q_recv.at[share - g, i],
-            ).start()
-        slab(m, c, sib, s_send.at[0, i], s_recv.at[0, i]).start()
+    def sib_piece(m, core, n):
+        return piece(m, core, n, sib, s_send.at[m, n], s_recv.at[m, n])
+
+    def group_piece(m, n, g):
+        to = {"grp": gbase + (gq + g) % share} if share > 1 else sib
+        return piece(m, c, n, to, q_send.at[g, m % nm, n], q_recv.at[m, n])
+
+    def hand_out(i, m):
+        for d in range(4):
+            n = (z // quarter + d) % 4
+            count = quarter - 1 if d == 0 else quarter
+            at = wb.at[m, c, pl.ds(0, count)]
+            pltpu.make_async_remote_copy(
+                src_ref=at,
+                dst_ref=at,
+                send_sem=w_send.at[i],
+                recv_sem=w_recv.at[i, n],
+                device_id=chip(z),
+                device_id_type=MESH,
+            ).wait_recv()
+            for g in range(1, share):
+                group_piece(m, n, g).start()
+            sib_piece(m, c, n).start()
+
+    def pass_on(m):
+        for n in range(4):
+            group_piece(m, n, 0).wait_recv()
+            sib_piece(m, c, n).start()
+
+    def mine(m):
+        return gq == m // nm
+
+    for m in range(3):
+        pl.when(mine(m))(functools.partial(hand_out, m % nm, m))
     gather_onward(xt, 0)
-    for g in range(1, share):
-        for i in range(nm):
-            m = ((gq + g) % share) * nm + i
-            slab(m, c, sib, q_send.at[g, i], q_recv.at[g, i]).wait_recv()
-            slab(m, c, sib, s_send.at[g, i], s_recv.at[g, i]).start()
+    if share > 1:
+        for m in range(3):
+            pl.when(jnp.logical_not(mine(m)))(functools.partial(pass_on, m))
 
     def widen(m, at):
         keep = left16.astype(F32).astype(BF16)
@@ -429,12 +456,9 @@
         a = (a + pltpu.roll(a, HEAD, 1)).reshape(nz, 8, 128)
         return a + pltpu.roll(a, ROWS, 1)
 
-    for g in range(share):
-        for i in range(nm):
-            m = ((gq + g) % share) * nm + i
-            slab(m, 1 - c, sib, s_send.at[g, i], s_recv.at[g, i]).wait_recv()
-
-    for m in range(4):
+    for m in range(3):
+        for n in range(4):
+            sib_piece(m, 1 - c, n).wait_recv()
         widen(m, m * 256)
 
     gather_wait(xt, 0)
@@ -456,6 +480,7 @@
             x2[s, :, :, half + 128 * m : half + 128 * m + 128] = jnp.where(
                 topk, pltpu.roll(one, ROWS, 1), two
             )
+    pl.when(mine(3))(functools.partial(hand_out, 3 % nm, 3))
     st_load.wait()
     scatter_all(yrecv, a_send.at[0], a_recv.at[0]).wait_recv()
 
@@ -525,8 +550,13 @@
         xm[res, own_k, :, 128 * j : 128 * j + 128] = tile.astype(BF16)
 
     gather_start(xm, 1)
+    if share > 1:
+        pl.when(jnp.logical_not(mine(3)))(functools.partial(pass_on, 3))
     gather_direct(xm, 1)
     gather_onward(xm, 1)
+    for n in range(4):
+        sib_piece(3, 1 - c, n).wait_recv()
+    widen(3, 768)
     gather_wait(xm, 1)
     co = fold(dot(rows_of(xm[...]), em[:, 768:1024]))
     xg[res, own_k] = jnp.where(
@@ -727,12 +757,13 @@
     gather_drain(xm, 1)
     gather_drain(xg, 2)
     for i in range(nm):
-        scatter_all(wb.at[gq * nm + i, c], w_send.at[i], w_recv.at[i]).wait_send()
-        slab(gq * nm + i, c, sib, s_send.at[0, i], s_recv.at[0, i]).wait_send()
+        scatter_all(wb.at[gq * nm + i, c], w_send.at[i], w_recv.at[i, 0]).wait_send()
         for g in range(1, share):
-            slab(gq * nm + i, c, sib, q_send.at[g, i], q_recv.at[g, i]).wait_send()
-            m = ((gq + g) % share) * nm + i
-            slab(m, c, sib, s_send.at[g, i], s_recv.at[g, i]).wait_send()
+            for n in range(4):
+                group_piece(gq * nm + i, n, g).wait_send()
+    for m in range(4):
+        for n in range(4):
+            sib_piece(m, c, n).wait_send()
     scatter_all(yrecv, a_send.at[0], a_recv.at[0]).wait_send()
     scatter_all(cb.at[c], a_send.at[2], a_recv.at[2]).wait_send()
     to_sib(cb.at[c], cb.at[c], 0).wait_send()
@@ -809,11 +840,11 @@
         pltpu.VMEM((nk, 8, half), BF16),
         dma((9,)),
         dma((nm,)),
-        dma((nm,)),
-        dma((share, nm)),
-        dma((share, nm)),
-        dma((share, nm)),
-        dma((share, nm)),
+        dma((nm, 4)),
+        dma((share, nm, 4)),
+        dma((4, 4)),
+        dma((4, 4)),
+        dma((4, 4)),
         dma((3, 7)),
         dma((3, 7)),
         dma((3, 3)),

time: 163 us -> 163 us (level)
  no operation moved by 1% of the time
where the time goes in v5:
time: 163 us
  Pallas kernels  156 us (96%)
  local copies, waits for them, and re-layouts  6.12 us (4%)
    pallas_call x1, Pallas kernels, step(): pl.pallas_call(functools.partial(kernel, nz, share), out_shape=(jax.Shape...  156 us
    unnamed x2, local copies, waits for them, and re-layouts  6.12 us

profile of v5, /device:TPU:46, one launch (start us, length us, event | category | flops | bytes accessed | tf_op | source)
XLA Modules:
  0.0 162.9 jit_solution(3686375487480883598)
XLA Ops:
  0.6 156.1 %shard_map.266 = (bf16[4,2048]{1,0:T(4,128)(2,1)}, f32[4,32,64,64]{3,2,1,0:T(8,128)}) custom-call(bf16[4,2048]{1,0:T(4,128)(2,1)} %tok_hbm.1, f32[4,32,64,64]{3,2,1,0:T(8,128)} %state_hbm.1, bf16[32,2048]{1,0:T(8,128)(2,1)} %wr_hbm.1, bf16[32,2048]{1,0:T(8,128)(2,1)} %wk_hbm.1, bf16[32,2048]{1,0:T(8,128)(2,1)} %wv_hbm.1, bf16[32,2048]{1,0:T(8,128)(2,1)} %wo_hbm.1, ...), custom_call_target="tpu_custom_call" | custom-call | tf_op jit(solution)/shard_map/pallas_call | solution.py:862
  156.8 1.3 copy.31
  158.1 4.8 %copy.32 = f32[4,32,64,64]{3,2,1,0:T(8,128)} copy(f32[4,32,64,64]{3,2,1,0:T(8,128)} %get-tuple-element.5) | data formatting | bytes 4194304

commit v6 on v5

--- a/solution.py
+++ b/solution.py
@@ -163,9 +163,9 @@
 
     bar = pltpu.get_barrier_semaphore()
 
-    @pl.loop(1, nz)
+    @pl.loop(0, nz - 1)
     def _(j):
-        pl.semaphore_signal(bar, inc=1, device_id=chip(z + j), device_id_type=MESH)
+        pl.semaphore_signal(bar, inc=1, device_id=chip(far_first(j)), device_id_type=MESH)
 
     pl.semaphore_signal(bar, inc=1, device_id=sib, device_id_type=MESH)
     for i in range(1, share):
@@ -368,6 +368,7 @@
 
     pl.semaphore_wait(bar, nz - 1 + 1 + share - 1)
 
+    gather_start(xt, 0)
     for i in range(nm):
         m = gq * nm + i
         scatter(
@@ -376,7 +377,6 @@
             w_send.at[i],
             w_recv.at[i, z // quarter],
         )
-    gather_start(xt, 0)
 
     gather_direct(xt, 0)
 
@@ -781,6 +781,23 @@
     for sem in used:
         step_sum(own_k, sem, sem).wait_send()
     st_store.wait()
+
+
+def hand_back(small, state, small_out, state_out, small_buf, buf, in_sem, out_sem):
+    pieces = [(small, small_buf, small_out)]
+    half = state.shape[1] // 2
+    for i in range(state.shape[0]):
+        for part in (pl.ds(0, half), pl.ds(half, half)):
+            pieces.append((state.at[i, part], buf.at[i, part], state_out.at[i, part]))
+    reads = [pltpu.make_async_copy(a, b, in_sem.at[i]) for i, (a, b, _) in enumerate(pieces)]
+    writes = [pltpu.make_async_copy(b, o, out_sem.at[i]) for i, (_, b, o) in enumerate(pieces)]
+    for cp in reads:
+        cp.start()
+    for read, write in zip(reads, writes):
+        read.wait()
+        write.start()
+    for cp in writes:
+        cp.wait()
 
 
 def step(nz, share, *args):
@@ -859,7 +876,7 @@
         dma((7,)),
         dma((SMALL,)),
     ]
-    return pl.pallas_call(
+    result, state_new = pl.pallas_call(
         functools.partial(kernel, nz, share),
         out_shape=(
             jax.ShapeDtypeStruct(tokens.shape, BF16),
@@ -872,6 +889,22 @@
             collective_id=0, has_side_effects=True, vmem_limit_bytes=56 * 1024 * 1024
         ),
     )(*operands)
+    return pl.pallas_call(
+        hand_back,
+        out_shape=(
+            jax.ShapeDtypeStruct(tokens.shape, BF16),
+            jax.ShapeDtypeStruct(state.shape, F32),
+        ),
+        in_specs=[hbm, hbm],
+        out_specs=(hbm, hbm),
+        scratch_shapes=[
+            pltpu.VMEM(tokens.shape, BF16),
+            pltpu.VMEM(state.shape, F32),
+            dma((1 + 2 * state.shape[0],)),
+            dma((1 + 2 * state.shape[0],)),
+        ],
+        compiler_params=pltpu.CompilerParams(vmem_limit_bytes=62 * 1024 * 1024),
+    )(result, state_new)
 
 
 def solution(mesh):

time: 163 us -> 159 us (0.975); the launches traced: 163 us -> 157 us
  local copies, waits for them, and re-layouts: 6.12 us -> 0 us
    unnamed x2 -> x0, local copies, waits for them, and re-layouts: 6.12 us -> none
    pallas_call x1, Pallas kernels: 156 us -> 152 us  [step(): pl.pallas_call(functools.partial(kernel, nz, share), out_shape=(jax.Shape...]
    pallas_call x0 -> x1, Pallas kernels: none -> 3.64 us  [step(): pl.pallas_call(hand_back, out_shape=(jax.ShapeDtypeStruct(tokens.shape, B...]
where the time goes in v6:
time: 159 us; the launch traced here: 157 us
  Pallas kernels  156 us (98%)
    pallas_call x1, Pallas kernels, step(): pl.pallas_call(functools.partial(kernel, nz, share), out_shape=(jax.Shape...  152 us
    pallas_call x1, Pallas kernels, step(): pl.pallas_call(hand_back, out_shape=(jax.ShapeDtypeStruct(tokens.shape, B...  3.64 us

profile of v6, /device:TPU:46, one launch (start us, length us, event | category | flops | bytes accessed | tf_op | source)
XLA Modules:
  0.0 156.5 jit_solution(6374943666290001210)
XLA Ops:
  0.6 152.2 %shard_map.266 = (bf16[4,2048]{1,0:T(4,128)(2,1)}, f32[4,32,64,64]{3,2,1,0:T(8,128)}) custom-call(bf16[4,2048]{1,0:T(4,128)(2,1)} %tok_hbm.1, f32[4,32,64,64]{3,2,1,0:T(8,128)} %state_hbm.1, bf16[32,2048]{1,0:T(8,128)(2,1)} %wr_hbm.1, bf16[32,2048]{1,0:T(8,128)(2,1)} %wk_hbm.1, bf16[32,2048]{1,0:T(8,128)(2,1)} %wv_hbm.1, bf16[32,2048]{1,0:T(8,128)(2,1)} %wo_hbm.1, ...), custom_call_target="tpu_custom_call" | custom-call | tf_op jit(solution)/shard_map/pallas_call | solution.py:879
  152.9 3.6 %shard_map.267 = (bf16[4,2048]{1,0:T(4,128)(2,1)}, f32[4,32,64,64]{3,2,1,0:T(8,128)}) custom-call(bf16[4,2048]{1,0:T(4,128)(2,1)} %get-tuple-element.4.small, f32[4,32,64,64]{3,2,1,0:T(8,128)} %get-tuple-element.5.state), custom_call_target="tpu_custom_call" | custom-call | tf_op jit(solution)/shard_map/pallas_call | solution.py:892

commit v7 on v6

--- a/solution.py
+++ b/solution.py
@@ -425,10 +425,10 @@
 
     for m in range(3):
         pl.when(mine(m))(functools.partial(hand_out, m % nm, m))
-    gather_onward(xt, 0)
     if share > 1:
         for m in range(3):
             pl.when(jnp.logical_not(mine(m)))(functools.partial(pass_on, m))
+    gather_onward(xt, 0)
 
     def widen(m, at):
         keep = left16.astype(F32).astype(BF16)

time: 159 us -> 159 us (level); the launches traced: 157 us -> 159 us
  Pallas kernels: 156 us -> 159 us
    pallas_call x1, Pallas kernels: 152 us -> 155 us  [step(): pl.pallas_call(functools.partial(kernel, nz, share), out_shape=(jax.Shape...]
where the time goes in v7:
time: 159 us
  Pallas kernels  159 us (100%)
    pallas_call x1, Pallas kernels, step(): pl.pallas_call(functools.partial(kernel, nz, share), out_shape=(jax.Shape...  155 us
    pallas_call x1, Pallas kernels, step(): pl.pallas_call(hand_back, out_shape=(jax.ShapeDtypeStruct(tokens.shape, B...  3.64 us

profile of v7, /device:TPU:46, one launch (start us, length us, event | category | flops | bytes accessed | tf_op | source)
XLA Modules:
  0.0 159.2 jit_solution(9615764261801712125)
XLA Ops:
  0.6 154.9 %shard_map.266 = (bf16[4,2048]{1,0:T(4,128)(2,1)}, f32[4,32,64,64]{3,2,1,0:T(8,128)}) custom-call(bf16[4,2048]{1,0:T(4,128)(2,1)} %tok_hbm.1, f32[4,32,64,64]{3,2,1,0:T(8,128)} %state_hbm.1, bf16[32,2048]{1,0:T(8,128)(2,1)} %wr_hbm.1, bf16[32,2048]{1,0:T(8,128)(2,1)} %wk_hbm.1, bf16[32,2048]{1,0:T(8,128)(2,1)} %wv_hbm.1, bf16[32,2048]{1,0:T(8,128)(2,1)} %wo_hbm.1, ...), custom_call_target="tpu_custom_call" | custom-call | tf_op jit(solution)/shard_map/pallas_call | solution.py:879
  155.6 3.6 %shard_map.267 = (bf16[4,2048]{1,0:T(4,128)(2,1)}, f32[4,32,64,64]{3,2,1,0:T(8,128)}) custom-call(bf16[4,2048]{1,0:T(4,128)(2,1)} %get-tuple-element.4.small, f32[4,32,64,64]{3,2,1,0:T(8,128)} %get-tuple-element.5.state), custom_call_target="tpu_custom_call" | custom-call | tf_op jit(solution)/shard_map/pallas_call | solution.py:892
